TPU v7x, 512 devices: a whole 4x8x8 slice. The times are simulated.
512 devices in a mesh: ep: 128 (over z, y, core), tp: 4 (over x).
Axes of the slice: x: 4, y: 8, z: 8, core: 2. Of those that a mesh axis runs over, the one named last changes fastest.
Arguments:
- residual_in: bfloat16 [256, 2048], P('ep'), may hold values from -6 to 6
- gla_state: float32 [256, 4, 256, 512], P('ep', 'tp'), may hold values from -6 to 6
- norm_gain: bfloat16 [2048], replicated, may hold values from 0.099609375 to 1.8984375
- w_query: bfloat16 [2048, 1024], P('ep', 'tp'), may hold values from -0.125 to 0.125
- w_key: bfloat16 [2048, 1024], P('ep', 'tp'), may hold values from -0.125 to 0.125
- w_value: bfloat16 [2048, 2048], P('ep', 'tp'), may hold values from -0.125 to 0.125
- w_decay: bfloat16 [2048, 1024], P('ep', 'tp'), may hold values from -0.5 to 0.5
- decay_bias: float32 [1024], P('tp'), may hold values from -40 to 8
- head_gain: bfloat16 [512], replicated, may hold values from 0.099609375 to 1.8984375
- w_output: bfloat16 [2048, 2048], P('tp', 'ep'), may hold values from -0.125 to 0.125
- ffn_gain: bfloat16 [2048], replicated, may hold values from 0.099609375 to 1.8984375
- router_group: bfloat16 [2048, 4], replicated, may hold values from -0.125 to 0.125
- router_expert: bfloat16 [128, 2048], replicated, may hold values from -0.125 to 0.125
- expert_ids: int32 [256, 2], replicated, may hold values from 0 to 127, all different within a row; in each aligned block of 256 rows (0 to 255, 256 to 511, ...) at most 16 rows name the same one
- w_gate: bfloat16 [128, 2048, 512], P('ep', None, 'tp'), may hold values from -0.125 to 0.125
- w_up: bfloat16 [128, 2048, 512], P('ep', None, 'tp'), may hold values from -0.125 to 0.125
- w_down: bfloat16 [128, 512, 2048], P('ep', 'tp'), may hold values from -0.75 to 0.75
Outputs:
- layer_out: bfloat16 [256, 2048], P('ep')
- new_state: float32 [256, 4, 256, 512], P('ep', 'tp')
Inputs may be any that keep to these rules, and one draw needn't show every extreme that they name: `expert_ids`: each row names 2 different experts; no expert is named by more than 16 rows of the whole batch, a bound that some block reaches.
All inputs are finite; a program needn't handle non-finite values.
Results may differ from a plain program's by a relative error of at most 0.023.
Values may be sent and summed in bfloat16 or wider, within the bound.
A program may use at most 64 MiB of HBM per device.

v0:
```python
import jax
import jax.numpy as jnp
from jax import lax
from jax.sharding import Mesh
from jax.sharding import PartitionSpec as P

CAP = 16
EP = ("ep_0", "ep_1", "ep_2")


EPSILON = 1e-06
GATE_SCALE = 16.0


def in_blocks(shard, dim, length):
    shape = shard.shape
    blocks = shard.reshape(*shape[:dim], length, shape[dim] // length, *shape[dim + 1 :])
    return jnp.moveaxis(blocks, dim, 0)


def summed_on_arrival(shard, axis, dim):
    blocks = in_blocks(shard, dim, lax.axis_size(axis))
    arrived = lax.all_to_all(blocks, axis, split_axis=0, concat_axis=0, tiled=True)
    return arrived.sum(axis=0)


def sum_by_axis(shard, axes, dim):
    far, near = axes
    own = summed_on_arrival(in_blocks(shard, dim, lax.axis_size(far)), near, dim + 1)
    return jnp.sum(lax.all_to_all(own, far, 0, 0, tiled=True), axis=0)


def from_everyone(shard, axis):
    copies = jnp.broadcast_to(shard, (lax.axis_size(axis), *shard.shape))
    return lax.all_to_all(copies, axis, split_axis=0, concat_axis=0, tiled=True)


def in_order(blocks, dim):
    shape = list(blocks.shape[1:])
    shape[dim] *= blocks.shape[0]
    return jnp.moveaxis(blocks, 0, dim).reshape(shape)


def whole_of(shard, axes, dim):
    far, near = axes
    blocks = from_everyone(from_everyone(shard, far), near)
    return in_order(blocks.swapaxes(0, 1).reshape(-1, *shard.shape), dim)


def taken_together(shard, axis):
    everything = from_everyone(shard, axis)
    return jnp.sum(everything.astype(jnp.float32), axis=0)


def sent_and_summed(shard, axis, dim):
    length = lax.axis_size(axis)
    blocks = lax.all_to_all(in_blocks(shard, dim, length), axis, 0, 0, tiled=True)
    return jnp.sum(blocks.astype(jnp.float32), axis=0)


def collect(shard, axis, dim):
    return in_order(from_everyone(shard, axis), dim)


def rms_scale(values, gain_vec):
    floats = values.astype(jnp.float32)
    return (
        floats
        * lax.rsqrt(jnp.mean(floats * floats, axis=-1, keepdims=True) + EPSILON)
        * gain_vec.astype(jnp.float32)
    )


def finish_part(hidden_res, moe_part, tp_index):
    part_cols = moe_part.shape[1]
    own_cols = lax.dynamic_slice_in_dim(hidden_res, tp_index * part_cols, part_cols, 1)
    return (own_cols.astype(jnp.float32) + moe_part).astype(jnp.bfloat16)


def on_device(
    residual_in,
    gla_state,
    norm_gain,
    w_query,
    w_key,
    w_value,
    w_decay,
    decay_bias,
    head_gain,
    w_output,
    ffn_gain,
    router_group,
    router_expert,
    expert_ids,
    w_gate,
    w_up,
    w_down,
):
    seq_rows = residual_in.shape[0]
    key_width = w_query.shape[1]
    value_width = w_value.shape[1]
    normed = rms_scale(residual_in, norm_gain).astype(jnp.bfloat16)
    columns = lax.all_to_all(normed, EP, split_axis=1, concat_axis=0, tiled=True)
    projected = sum_by_axis(
        jnp.concatenate(
            [
                jnp.dot(columns, w_query, preferred_element_type=jnp.float32),
                jnp.dot(columns, w_key, preferred_element_type=jnp.float32),
                jnp.dot(columns, w_value, preferred_element_type=jnp.float32),
                jnp.dot(columns, w_decay, preferred_element_type=jnp.float32),
            ],
            axis=1,
        ),
        (("ep_0", "ep_1"), "ep_2"),
        0,
    )
    query_rows = projected[:, :key_width].astype(jnp.bfloat16)
    key_rows = projected[:, key_width : 2 * key_width].astype(jnp.bfloat16)
    value_rows = projected[:, 2 * key_width : 2 * key_width + value_width].astype(jnp.bfloat16)
    decay_pre = projected[:, 2 * key_width + value_width :]
    log_decay = jax.nn.log_sigmoid(decay_pre + decay_bias) / GATE_SCALE
    query_float = lax.optimization_barrier(query_rows).astype(jnp.float32) * key_width ** (-0.5)
    key_float = lax.optimization_barrier(key_rows).astype(jnp.float32)
    value_float = lax.optimization_barrier(value_rows).astype(jnp.float32)
    old_state = gla_state[:, 0]
    new_state = (
        jnp.exp(log_decay)[:, :, None] * old_state + key_float[:, :, None] * value_float[:, None, :]
    )
    read_out = jnp.einsum("tk,tkv->tv", query_float, new_state, precision=lax.Precision.HIGHEST)
    gated_heads = rms_scale(read_out, head_gain).astype(jnp.bfloat16)
    partial_out = jnp.dot(
        whole_of(gated_heads, (("ep_0", "ep_1"), "ep_2"), 0),
        w_output,
        preferred_element_type=jnp.float32,
    ).astype(jnp.bfloat16)
    returned = lax.all_to_all(partial_out, EP, split_axis=0, concat_axis=1, tiled=True)
    attention = taken_together(returned.astype(jnp.float32).astype(jnp.bfloat16), "tp").astype(
        jnp.float32
    )
    hidden_res = (residual_in.astype(jnp.float32) + attention).astype(jnp.bfloat16)
    moe_in = rms_scale(hidden_res, ffn_gain).astype(jnp.bfloat16)
    expert = lax.axis_index(EP)
    is_named = jnp.any(expert_ids == expert, axis=1)
    slot_of = jnp.cumsum(is_named.astype(jnp.int32)) - 1
    slot_index = jnp.arange(CAP, dtype=jnp.int32)
    select_int = (is_named[None, :] & (slot_of[None, :] == slot_index[:, None])).astype(jnp.int32)
    select_bf = select_int.astype(jnp.bfloat16)
    slot_rows = jnp.dot(
        select_bf,
        whole_of(moe_in, (("ep_0", "ep_1"), "ep_2"), 0),
        preferred_element_type=jnp.float32,
    ).astype(jnp.bfloat16)
    slot_ids = jnp.sum(select_int[:, :, None] * expert_ids[None, :, :], axis=1)
    rival_ids = jnp.where(slot_ids[:, 0] == expert, slot_ids[:, 1], slot_ids[:, 0])
    group_logits = jnp.dot(slot_rows, router_group, preferred_element_type=jnp.float32)
    per_group = router_expert.shape[0] // router_group.shape[1]
    own_group = jnp.arange(router_group.shape[1], dtype=jnp.int32) == expert // per_group
    group_logit = jnp.sum(
        jnp.where(own_group[None, :], group_logits, jnp.zeros_like(group_logits)), axis=1
    )
    group_share = 1.0 / jnp.sum(jnp.exp(group_logits - group_logit[:, None]), axis=1)
    chosen = jnp.dot(slot_rows, router_expert[expert], preferred_element_type=jnp.float32)
    rival_logit = jnp.einsum(
        "cd,cd->c", slot_rows, router_expert[rival_ids], preferred_element_type=jnp.float32
    )
    slot_weight = group_share * jax.nn.sigmoid(chosen - rival_logit)
    gate_out = jnp.dot(slot_rows, w_gate[0], preferred_element_type=jnp.float32)
    up_out = jnp.dot(slot_rows, w_up[0], preferred_element_type=jnp.float32)
    hidden = (jax.nn.silu(gate_out) * up_out).astype(jnp.bfloat16)
    output = jnp.dot(hidden, w_down[0], preferred_element_type=jnp.float32)
    select_float = select_int.astype(jnp.float32)
    width_piece = sent_and_summed(output.astype(jnp.bfloat16), "tp", 1)
    weighted_piece = width_piece * slot_weight[:, None]
    piece_cols = weighted_piece.shape[1]
    outgoing = jnp.dot(select_float.T, weighted_piece, precision=lax.Precision.HIGHEST)
    owners = outgoing.shape[0] // seq_rows
    outgoing = outgoing.reshape(owners, seq_rows, piece_cols)
    arrived = lax.all_to_all(
        outgoing.astype(jnp.bfloat16), EP, split_axis=0, concat_axis=0, tiled=True
    ).astype(outgoing.dtype)
    moe_piece = jnp.sum(arrived, axis=0)
    layer_piece = finish_part(hidden_res, moe_piece, lax.axis_index("tp"))
    layer_out = collect(layer_piece, "tp", 1)
    return (layer_out, new_state[:, None])


def solution(mesh):
    torus = Mesh(mesh.devices.reshape(8, 8, 2, mesh.shape["tp"]), ("ep_0", "ep_1", "ep_2", "tp"))
    in_specs = (
        P(EP, None),
        P(EP, "tp", None, None),
        P(),
        P(EP, "tp"),
        P(EP, "tp"),
        P(EP, "tp"),
        P(EP, "tp"),
        P("tp"),
        P(),
        P("tp", EP),
        P(),
        P(),
        P(),
        P(),
        P(EP, None, "tp"),
        P(EP, None, "tp"),
        P(EP, "tp", None),
    )
    out_specs = (P(EP, None), P(EP, "tp", None, None))
    return jax.shard_map(
        on_device, mesh=torus, in_specs=in_specs, out_specs=out_specs, check_vma=False
    )
```

profile of v0, /device:TPU:1, one launch (start us, length us, event | category | flops | bytes accessed | tf_op | source)
XLA Modules:
  0.0 201.6 jit_solution(11595900406696143059)
XLA Ops:
  0.7 0.7 convert_element_type.96
  1.4 0.8 fusion.24
  2.2 0.8 fusion.26
  3.0 0.1 all_to_all.58
  3.2 29.7 %all_to_all.88 = bf16[2,128,16]{2,0,1:T(2,128)(2,1)S(1)} all-to-all(bf16[2,128,16]{2,0,1:T(2,128)(2,1)S(1)} %copy.63), channel_id=1, replica_groups=mesh['ep_0'=8,'ep_1'=8,'ep_2'=2,'tp'=4] {'ep_0','ep_1','ep_2'}, dimensions={1} | all-to-all | bytes 16384 | tf_op jit(solution)/shard_map/all_to_all | solution.py:103
  32.9 0.9 fusion.62
  33.8 0.8 fusion.60
  34.7 0.1 fusion.61
  34.9 0.2 fusion.63
  35.0 0.1 pad_maximum_fusion
  35.1 0.8 reshape_reshape.9
  35.9 0.1 copy.94
  36.0 5.0 %all_to_all.89 = f32[2,64,2,1280]{3,2,1,0:T(2,128)S(1)} all-to-all(f32[2,64,2,1280]{3,2,1,0:T(2,128)S(1)} %bitcast.85), channel_id=1, replica_groups=mesh['ep_0'=8,'ep_1'=8,'ep_2'=2,'tp'=4] {'ep_2'}, dimensions={0} | all-to-all | bytes 2621440 | tf_op jit(solution)/shard_map/all_to_all | solution.py:23
  41.0 2.0 %reduce_sum.100 = f32[64,2,1280]{2,1,0:T(2,128)} reduce(f32[2,64,2,1280]{3,2,1,0:T(2,128)S(1)} %all_to_all.89, f32[]{:T(128)} %constant.26.clone.1), dimensions={0}, to_apply=%region_1.0 | reduce | flops 163840 | bytes 1966084 | tf_op jit(solution)/shard_map/reduce_sum | solution.py:24
  43.0 4.8 %all-to-all-start.2 = ((f32[64,2,1280]{2,1,0:T(2,128)}), f32[64,2,1280]{2,1,0:T(2,128)S(1)}, u32[]{:S(2)}, u32[]{:S(2)}) async-start(f32[64,2,1280]{2,1,0:T(2,128)} %reduce_sum.100), calls=%async_computation.2 | async-start | bytes 1310720 | tf_op jit(solution)/shard_map/all_to_all | solution.py:30
  47.8 20.1 %all-to-all-done.2 = f32[64,2,1280]{2,1,0:T(2,128)S(1)} async-done(((f32[64,2,1280]{2,1,0:T(2,128)}), f32[64,2,1280]{2,1,0:T(2,128)S(1)}, u32[]{:S(2)}, u32[]{:S(2)}) %all-to-all-start.2) | async-done | bytes 655392 | tf_op jit(solution)/shard_map/all_to_all | solution.py:30
  67.9 0.2 reduce_sum.101
  68.3 0.8 fusion.8
  69.1 0.1 fusion.46
  69.3 0.7 broadcast_in_dim.19
  70.0 7.0 %all-to-all-start.3 = ((bf16[64,2,512]{2,1,0:T(2,128)(2,1)}), bf16[64,2,512]{2,1,0:T(2,128)(2,1)S(1)}, u32[]{:S(2)}, u32[]{:S(2)}) async-start(bf16[64,2,512]{2,1,0:T(2,128)(2,1)} %broadcast_in_dim.19), calls=%async_computation.3 | async-start | bytes 262144 | tf_op jit(solution)/shard_map/all_to_all | solution.py:35
  77.0 11.5 %all-to-all-done.3 = bf16[64,2,512]{2,1,0:T(2,128)(2,1)S(1)} async-done(((bf16[64,2,512]{2,1,0:T(2,128)(2,1)}), bf16[64,2,512]{2,1,0:T(2,128)(2,1)S(1)}, u32[]{:S(2)}, u32[]{:S(2)}) %all-to-all-start.3) | async-done | bytes 131104 | tf_op jit(solution)/shard_map/all_to_all | solution.py:35
  88.5 0.1 broadcast_in_dim.20
  88.7 6.5 %all_to_all.90 = bf16[2,64,2,512]{3,2,1,0:T(2,128)(2,1)S(1)} all-to-all(bf16[2,64,2,512]{3,2,1,0:T(2,128)(2,1)S(1)} %broadcast_in_dim.20), channel_id=1, replica_groups=mesh['ep_0'=8,'ep_1'=8,'ep_2'=2,'tp'=4] {'ep_2'}, dimensions={0} | all-to-all | bytes 524288 | tf_op jit(solution)/shard_map/all_to_all | solution.py:35
  95.1 0.2 copy.69
  95.3 0.1 reshape_reshape.10
  95.4 0.2 convolution_convert_fusion.3
  95.6 0.8 copy.70
  96.4 5.5 %all-to-all-start.5 = ((bf16[128,2,16]{2,1,0:T(2,128)(2,1)}), bf16[128,2,16]{2,1,0:T(2,128)(2,1)S(1)}, u32[]{:S(2)}, u32[]{:S(2)}) async-start(bf16[128,2,16]{2,1,0:T(2,128)(2,1)} %bitcast.8), calls=%async_computation.5 | async-start | bytes 131072 | tf_op jit(solution)/shard_map/all_to_all | solution.py:136
  101.9 11.5 %all-to-all-done.5 = bf16[128,2,16]{2,1,0:T(2,128)(2,1)S(1)} async-done(((bf16[128,2,16]{2,1,0:T(2,128)(2,1)}), bf16[128,2,16]{2,1,0:T(2,128)(2,1)S(1)}, u32[]{:S(2)}, u32[]{:S(2)}) %all-to-all-start.5) | async-done | bytes 8224 | tf_op jit(solution)/shard_map/all_to_all | solution.py:136
  113.4 0.1 all_to_all.69
  113.5 0.6 broadcast_in_dim.21
  114.2 4.0 %all-to-all-start.6 = ((bf16[4,2,2048]{2,1,0:T(2,128)(2,1)}), bf16[4,2,2048]{2,1,0:T(2,128)(2,1)S(1)}, u32[]{:S(2)}, u32[]{:S(2)}) async-start(bf16[4,2,2048]{2,1,0:T(2,128)(2,1)} %broadcast_in_dim.21), calls=%async_computation.6 | async-start | bytes 65536 | tf_op jit(solution)/shard_map/all_to_all | solution.py:35
  118.2 0.3 reduce-window.9
  118.6 3.9 %all-to-all-done.6 = bf16[4,2,2048]{2,1,0:T(2,128)(2,1)S(1)} async-done(((bf16[4,2,2048]{2,1,0:T(2,128)(2,1)}), bf16[4,2,2048]{2,1,0:T(2,128)(2,1)S(1)}, u32[]{:S(2)}, u32[]{:S(2)}) %all-to-all-start.6) | async-done | bytes 32800 | tf_op jit(solution)/shard_map/all_to_all | solution.py:35
  122.6 0.1 fusion.21
  122.8 1.1 broadcast_in_dim.22
  123.9 4.8 %all-to-all-start.7 = ((bf16[64,2,2048]{2,1,0:T(2,128)(2,1)}), bf16[64,2,2048]{2,1,0:T(2,128)(2,1)S(1)}, u32[]{:S(2)}, u32[]{:S(2)}) async-start(bf16[64,2,2048]{2,1,0:T(2,128)(2,1)} %broadcast_in_dim.22), calls=%async_computation.7 | async-start | bytes 1048576 | tf_op jit(solution)/shard_map/all_to_all | solution.py:35
  128.7 0.1 slice_reduce_fusion
  128.9 0.1 multiply_reduce_fusion
  129.0 0.6 gather_fusion
  129.7 14.8 %all-to-all-done.7 = bf16[64,2,2048]{2,1,0:T(2,128)(2,1)S(1)} async-done(((bf16[64,2,2048]{2,1,0:T(2,128)(2,1)}), bf16[64,2,2048]{2,1,0:T(2,128)(2,1)S(1)}, u32[]{:S(2)}, u32[]{:S(2)}) %all-to-all-start.7) | async-done | bytes 524320 | tf_op jit(solution)/shard_map/all_to_all | solution.py:35
  144.5 0.5 broadcast_in_dim.23
  145.0 9.1 %all_to_all.91 = bf16[2,64,2,2048]{3,2,1,0:T(2,128)(2,1)S(1)} all-to-all(bf16[2,64,2,2048]{3,2,1,0:T(2,128)(2,1)S(1)} %broadcast_in_dim.23), channel_id=1, replica_groups=mesh['ep_0'=8,'ep_1'=8,'ep_2'=2,'tp'=4] {'ep_2'}, dimensions={0} | all-to-all | bytes 2097152 | tf_op jit(solution)/shard_map/all_to_all | solution.py:35
  154.1 2.2 %copy.73 = bf16[64,2,2,2048]{3,2,1,0:T(2,128)(2,1)} copy(bf16[64,2,2,2048]{3,2,0,1:T(2,128)(2,1)S(1)} %bitcast.86) | data formatting | bytes 2097152 | tf_op jit(solution)/shard_map/transpose | solution.py:47
  156.3 1.5 reshape_reshape.11
  157.8 0.4 fusion.19
  158.2 1.2 fusion.14
  159.4 1.4 convolution_convert_fusion
  160.8 0.7 copy.95
  161.5 3.3 %all-to-all-start.9 = ((bf16[4,16,512]{2,1,0:T(8,128)(2,1)}), bf16[4,16,512]{2,1,0:T(8,128)(2,1)S(1)}, u32[]{:S(2)}, u32[]{:S(2)}) async-start(bf16[4,16,512]{2,1,0:T(8,128)(2,1)} %bitcast.84), calls=%async_computation.9 | async-start | bytes 131072 | tf_op jit(solution)/shard_map/all_to_all | solution.py:57
  164.8 0.1 select_reduce_fusion
  165.0 0.1 fusion.6
  165.1 4.1 %all-to-all-done.9 = bf16[4,16,512]{2,1,0:T(8,128)(2,1)S(1)} async-done(((bf16[4,16,512]{2,1,0:T(8,128)(2,1)}), bf16[4,16,512]{2,1,0:T(8,128)(2,1)S(1)}, u32[]{:S(2)}, u32[]{:S(2)}) %all-to-all-start.9) | async-done | bytes 65568 | tf_op jit(solution)/shard_map/all_to_all | solution.py:57
  169.2 0.6 convolution_convert_fusion.2
  169.9 0.8 convert_element_type.120
  170.7 6.8 %all-to-all-start.10 = ((bf16[128,2,512]{2,1,0:T(2,128)(2,1)}), bf16[128,2,512]{2,1,0:T(2,128)(2,1)S(1)}, u32[]{:S(2)}, u32[]{:S(2)}) async-start(bf16[128,2,512]{2,1,0:T(2,128)(2,1)} %convert_element_type.120), calls=%async_computation.10 | async-start | bytes 524288 | tf_op jit(solution)/shard_map/all_to_all | solution.py:178
  177.5 15.2 %all-to-all-done.10 = bf16[128,2,512]{2,1,0:T(2,128)(2,1)S(1)} async-done(((bf16[128,2,512]{2,1,0:T(2,128)(2,1)}), bf16[128,2,512]{2,1,0:T(2,128)(2,1)S(1)}, u32[]{:S(2)}, u32[]{:S(2)}) %all-to-all-start.10) | async-done | bytes 262176 | tf_op jit(solution)/shard_map/all_to_all | solution.py:178
  192.7 0.3 convert_reduce_fusion
  193.0 0.6 broadcast_in_dim.29
  193.6 3.2 %all-to-all-start.11 = ((bf16[4,2,512]{2,1,0:T(2,128)(2,1)}), bf16[4,2,512]{2,1,0:T(2,128)(2,1)S(1)}, u32[]{:S(2)}, u32[]{:S(2)}) async-start(bf16[4,2,512]{2,1,0:T(2,128)(2,1)} %broadcast_in_dim.29), calls=%async_computation.11 | async-start | bytes 16384 | tf_op jit(solution)/shard_map/all_to_all | solution.py:35
  196.9 1.2 multiply_add_fusion
  198.0 3.0 %all-to-all-done.11 = bf16[4,2,512]{2,1,0:T(2,128)(2,1)S(1)} async-done(((bf16[4,2,512]{2,1,0:T(2,128)(2,1)}), bf16[4,2,512]{2,1,0:T(2,128)(2,1)S(1)}, u32[]{:S(2)}, u32[]{:S(2)}) %all-to-all-start.11) | async-done | bytes 8224 | tf_op jit(solution)/shard_map/all_to_all | solution.py:35
  201.0 0.6 copy.97
  (53 shorter events, 0.7 us)
Async XLA Ops:
  0.6 128.4 %copy-start = (bf16[128,2048]{1,0:T(8,128)(2,1)S(1)}, bf16[128,2048]{1,0:T(8,128)(2,1)}, u32[]{:S(2)}) copy-start(bf16[128,2048]{1,0:T(8,128)(2,1)} %param.29) | copy-start | bytes 1572868
  0.6 34.0 %copy-start.6 = (bf16[16,256]{1,0:T(8,128)(2,1)S(1)}, bf16[16,256]{1,0:T(8,128)(2,1)}, u32[]{:S(2)}) copy-start(bf16[16,256]{1,0:T(8,128)(2,1)} %param.21) | copy-start | bytes 24580
  0.7 34.2 %copy-start.7 = (bf16[16,256]{1,0:T(8,128)(2,1)S(1)}, bf16[16,256]{1,0:T(8,128)(2,1)}, u32[]{:S(2)}) copy-start(bf16[16,256]{1,0:T(8,128)(2,1)} %param.23) | copy-start | bytes 24580
  41.0 6.8 %copy-start.9 = (bf16[512]{0:T(512)(128)(2,1)S(1)}, bf16[512]{0:T(512)(128)(2,1)}, u32[]{:S(2)}) copy-start(bf16[512]{0:T(512)(128)(2,1)} %param.25) | copy-start | bytes 3076
  43.0 25.2 %copy-start.10 = (f32[256]{0:T(256)S(1)}, f32[256]{0:T(256)}, u32[]{:S(2)}) copy-start(f32[256]{0:T(256)} %param.24) | copy-start | bytes 3076
  43.0 25.2 %copy-start.1 = (f32[2,1,256,512]{3,2,1,0:T(8,128)S(1)}, f32[2,1,256,512]{3,2,1,0:T(8,128)}, u32[]{:S(2)}) copy-start(f32[2,1,256,512]{3,2,1,0:T(8,128)} %param.18) | copy-start | bytes 3145732
  43.0 24.9 %all-to-all-start.2 = ((f32[64,2,1280]{2,1,0:T(2,128)}), f32[64,2,1280]{2,1,0:T(2,128)S(1)}, u32[]{:S(2)}, u32[]{:S(2)}) async-start(f32[64,2,1280]{2,1,0:T(2,128)} %reduce_sum.100), calls=%async_computation.2 | async-start | bytes 1310720 | tf_op jit(solution)/shard_map/all_to_all | solution.py:30
  69.1 26.4 %copy-start.4 = (bf16[512,16]{0,1:T(8,128)(2,1)S(1)}, bf16[512,16]{0,1:T(8,128)(2,1)}, u32[]{:S(2)}) copy-start(bf16[512,16]{0,1:T(8,128)(2,1)} %param.26) | copy-start | bytes 49156
  70.0 31.9 %copy-start.5 = (s32[256,2]{0,1:T(2,128)S(1)}, s32[256,2]{0,1:T(2,128)}, u32[]{:S(2)}) copy-start(s32[256,2]{0,1:T(2,128)} %param.30) | copy-start | bytes 6148
  70.0 18.5 %all-to-all-start.3 = ((bf16[64,2,512]{2,1,0:T(2,128)(2,1)}), bf16[64,2,512]{2,1,0:T(2,128)(2,1)S(1)}, u32[]{:S(2)}, u32[]{:S(2)}) async-start(bf16[64,2,512]{2,1,0:T(2,128)(2,1)} %broadcast_in_dim.19), calls=%async_computation.3 | async-start | bytes 262144 | tf_op jit(solution)/shard_map/all_to_all | solution.py:35
  77.0 41.2 %copy-start.8 = (bf16[2048]{0:T(1024)(128)(2,1)S(1)}, bf16[2048]{0:T(1024)(128)(2,1)}, u32[]{:S(2)}) copy-start(bf16[2048]{0:T(1024)(128)(2,1)} %param.27) | copy-start | bytes 12292
  88.7 33.9 %copy-start.3 = (bf16[2,2048]{1,0:T(2,128)(2,1)S(1)}, bf16[2,2048]{1,0:T(2,128)(2,1)}, u32[]{:S(2)}) copy-start(bf16[2,2048]{1,0:T(2,128)(2,1)} %param.17) | copy-start | bytes 24580
  96.4 17.0 %all-to-all-start.5 = ((bf16[128,2,16]{2,1,0:T(2,128)(2,1)}), bf16[128,2,16]{2,1,0:T(2,128)(2,1)S(1)}, u32[]{:S(2)}, u32[]{:S(2)}) async-start(bf16[128,2,16]{2,1,0:T(2,128)(2,1)} %bitcast.8), calls=%async_computation.5 | async-start | bytes 131072 | tf_op jit(solution)/shard_map/all_to_all | solution.py:136
  114.2 8.3 %all-to-all-start.6 = ((bf16[4,2,2048]{2,1,0:T(2,128)(2,1)}), bf16[4,2,2048]{2,1,0:T(2,128)(2,1)S(1)}, u32[]{:S(2)}, u32[]{:S(2)}) async-start(bf16[4,2,2048]{2,1,0:T(2,128)(2,1)} %broadcast_in_dim.21), calls=%async_computation.6 | async-start | bytes 65536 | tf_op jit(solution)/shard_map/all_to_all | solution.py:35
  123.9 20.6 %all-to-all-start.7 = ((bf16[64,2,2048]{2,1,0:T(2,128)(2,1)}), bf16[64,2,2048]{2,1,0:T(2,128)(2,1)S(1)}, u32[]{:S(2)}, u32[]{:S(2)}) async-start(bf16[64,2,2048]{2,1,0:T(2,128)(2,1)} %broadcast_in_dim.22), calls=%async_computation.7 | async-start | bytes 1048576 | tf_op jit(solution)/shard_map/all_to_all | solution.py:35
  157.8 1.6 copy-start.2
  158.2 6.6 %copy-start.11 = (bf16[2048,4]{0,1:T(4,128)(2,1)S(1)}, bf16[2048,4]{0,1:T(4,128)(2,1)}, u32[]{:S(2)}) copy-start(bf16[2048,4]{0,1:T(4,128)(2,1)} %param.28) | copy-start | bytes 49156
  161.5 7.7 %all-to-all-start.9 = ((bf16[4,16,512]{2,1,0:T(8,128)(2,1)}), bf16[4,16,512]{2,1,0:T(8,128)(2,1)S(1)}, u32[]{:S(2)}, u32[]{:S(2)}) async-start(bf16[4,16,512]{2,1,0:T(8,128)(2,1)} %bitcast.84), calls=%async_computation.9 | async-start | bytes 131072 | tf_op jit(solution)/shard_map/all_to_all | solution.py:57
  170.7 22.0 %all-to-all-start.10 = ((bf16[128,2,512]{2,1,0:T(2,128)(2,1)}), bf16[128,2,512]{2,1,0:T(2,128)(2,1)S(1)}, u32[]{:S(2)}, u32[]{:S(2)}) async-start(bf16[128,2,512]{2,1,0:T(2,128)(2,1)} %convert_element_type.120), calls=%async_computation.10 | async-start | bytes 524288 | tf_op jit(solution)/shard_map/all_to_all | solution.py:178
  193.6 7.4 %all-to-all-start.11 = ((bf16[4,2,512]{2,1,0:T(2,128)(2,1)}), bf16[4,2,512]{2,1,0:T(2,128)(2,1)S(1)}, u32[]{:S(2)}, u32[]{:S(2)}) async-start(bf16[4,2,512]{2,1,0:T(2,128)(2,1)} %broadcast_in_dim.29), calls=%async_computation.11 | async-start | bytes 16384 | tf_op jit(solution)/shard_map/all_to_all | solution.py:35
where the time goes:
time: 203 us; the launch traced here: 202 us
  waiting for transfers between devices  84.1 us (41%)
  blocking collectives  50.2 us (25%)
  starting transfers between devices  39.4 us (19%)
  local copies, waits for them, and re-layouts  12.6 us (6%)
  other arithmetic  7.32 us (4%)
  matrix products  6.88 us (3%)
    all_to_all x4, waiting for transfers between devices, from_everyone(): return lax.all_to_all(copies, axis, split_axis=0, concat_axis=0, tiled=True)  33.2 us
    all_to_all x1, blocking collectives, on_device(): lax.all_to_all(normed, EP, split_axis=1, concat_axis=0, tiled=True)  29.7 us
    all_to_all x1, waiting for transfers between devices, sum_by_axis(): return jnp.sum(lax.all_to_all(own, far, 0, 0, tiled=True), axis=0)  20.1 us
    all_to_all x4, starting transfers between devices, from_everyone(): return lax.all_to_all(copies, axis, split_axis=0, concat_axis=0, tiled=True)  19 us
    all_to_all x2, blocking collectives, from_everyone(): return lax.all_to_all(copies, axis, split_axis=0, concat_axis=0, tiled=True)  15.6 us
    all_to_all x1, waiting for transfers between devices, on_device(): lax.all_to_all(outgoing.astype(jnp.bfloat16), EP, split_axis=0, concat_ax...  15.2 us
    all_to_all x1, waiting for transfers between devices, on_device(): lax.all_to_all(partial_out, EP, split_axis=0, concat_axis=1, tiled=True)  11.5 us
    all_to_all x1, starting transfers between devices, on_device(): lax.all_to_all(outgoing.astype(jnp.bfloat16), EP, split_axis=0, concat_ax...  6.79 us
  transfers between devices with their start and end apart: 8, of which 8 were waited for; matrix products, arithmetic and copies ran while one was open for 1% of the time, Pallas kernels for 0%

commit v1 on v0

v1 whole, which is shorter than its diff:
```python
import functools
import types

import jax
import jax.numpy as jnp
from jax import lax
from jax.experimental import pallas as pl
from jax.experimental.pallas import tpu as pltpu
from jax.sharding import Mesh
from jax.sharding import PartitionSpec as P

CAP = 16
EPSILON = 1e-06
GATE_SCALE = 16.0
AXES = ("z", "y", "c", "x")
EP = ("z", "y", "c")
MESH = pl.DeviceIdType.MESH
BF16 = jnp.bfloat16
F32 = jnp.float32

(
    PROJ_W,
    PROJ_T,
    OUT_W,
    PROJ_SUM,
    HEADS,
    HEAD_SUM,
    GATHER,
    PICKED,
    GATE_W,
    DOWN_W,
    GATE_SUM,
    MERGE,
    COMBINE,
    QUARTERS,
    EXCHANGES,
) = range(15)


def rounds(n, offset):
    return min(offset % n, -offset % n)


def rms_scale(values, gain):
    mean = jnp.mean(values * values, axis=-1, keepdims=True)
    return values * lax.rsqrt(mean + EPSILON) * gain


def matmul(a, b):
    return jnp.dot(a, b, preferred_element_type=F32)


def matmul_t(a, b):
    return lax.dot_general(a, b, (((1,), (1,)), ((), ())), preferred_element_type=F32)


def layer_kernel(
    s,
    residual,
    norm_gain,
    w_query,
    w_key,
    w_value,
    w_decay,
    decay_bias,
    state,
    head_gain,
    w_output_t,
    ffn_gain,
    router_group_t,
    router_expert,
    ids_t,
    w_gate,
    w_up,
    w_down,
    layer_out,
    alpha_out,
    key_out,
    value_out,
    v_residual,
    v_norm_gain,
    v_bias,
    v_head_gain,
    v_ffn_gain,
    v_ids,
    v_state,
    v_router,
    v_group,
    w_own,
    w_row,
    normed_out,
    normed_in,
    out_w,
    sums_out,
    sums_in,
    heads,
    head_out,
    head_in,
    moe_in,
    hidden_q,
    gathered,
    picked_out,
    picked_in,
    gate_w,
    down_w,
    partial,
    merge_out,
    merge_in,
    combine_out,
    combine_in,
    quarters,
    v_alpha,
    v_key,
    v_value,
    v_layer,
    load_sem,
    store_sem,
    send_sem,
    recv_sem,
    plane_sem,
):
    z, y, c, x = (lax.axis_index(a) for a in AXES)
    other_c = 1 - c
    row = y * s.C + c
    plane = z * s.Y + y
    expert = plane * s.C + c
    half_w = s.half

    def at(dz=0, dy=0, dc=0, dx=0):
        return (
            lax.rem(z + dz, s.Z) if dz else z,
            lax.rem(y + dy, s.Y) if dy else y,
            lax.rem(c + dc, s.C) if dc else c,
            lax.rem(x + dx, s.X) if dx else x,
        )

    def ordered(offsets):
        def far(o):
            return -(rounds(s.Z, o[0]) + rounds(s.Y, o[1]) + rounds(s.X, o[3]))

        return sorted((o for o in offsets if any(o)), key=far)

    z_c = ordered((i, 0, k, 0) for i in range(s.Z) for k in range(s.C))
    y_c = ordered((0, i, k, 0) for i in range(s.Y) for k in range(s.C))
    z_only = ordered((i, 0, 0, 0) for i in range(s.Z))
    z_x = ordered((i, 0, 0, j) for i in range(s.Z) for j in range(s.X))
    z_y = ordered((i, j, 0, 0) for i in range(s.Z) for j in range(s.Y))
    x_only = ordered((0, 0, 0, i) for i in range(s.X))
    partner = at(dc=1)

    def send(which, src, dst, device):
        pltpu.make_async_remote_copy(
            src_ref=src,
            dst_ref=dst,
            send_sem=send_sem.at[which],
            recv_sem=recv_sem.at[which],
            device_id=device,
            device_id_type=MESH,
        ).start()

    def all_of(which, ref):
        return pltpu.make_async_remote_copy(
            src_ref=ref,
            dst_ref=ref,
            send_sem=send_sem.at[which],
            recv_sem=recv_sem.at[which],
            device_id=partner,
            device_id_type=MESH,
        )

    loads = []

    def load(src, dst):
        copy = pltpu.make_async_copy(src, dst, load_sem.at[len(loads)])
        loads.append(copy)
        copy.start()
        return copy

    k = s.dkh
    ld_weights = [
        load(w_query, w_own.at[0, :, pl.ds(0, k)]),
        load(w_key, w_own.at[0, :, pl.ds(k, k)]),
        load(w_decay.at[:, pl.ds(0, k // 2)], w_own.at[0, :, pl.ds(2 * k, k // 2)]),
        load(w_decay.at[:, pl.ds(k // 2, k // 2)], w_own.at[1, :, pl.ds(0, k // 2)]),
        load(w_value, w_own.at[1, :, pl.ds(k // 2, s.dvh)]),
    ]
    ld_residual = [load(residual, v_residual), load(norm_gain, v_norm_gain)]
    ld_ids = load(ids_t, v_ids)
    own_rows = pl.ds(pl.multiple_of(row * s.rows, s.rows), s.rows)
    own_q = pl.ds(pl.multiple_of(x * s.dq, s.dq), s.dq)
    own_f = pl.ds(pl.multiple_of(x * s.fh, s.fh), s.fh)
    own_f2 = pl.ds(pl.multiple_of(s.ff + x * s.fh, s.fh), s.fh)
    ld_state = [load(decay_bias, v_bias), load(head_gain, v_head_gain), load(state, v_state)]
    ld_out_w = [load(w_output_t, out_w.at[own_rows, :])]
    ld_ffn = [load(ffn_gain, v_ffn_gain)]
    ld_moe = [
        load(w_gate.at[own_q, :], gate_w.at[:, own_f]),
        load(w_up.at[own_q, :], gate_w.at[:, own_f2]),
        load(w_down.at[:, own_q], down_w.at[own_f, :]),
        load(router_expert.at[:, own_q], v_router),
        load(router_group_t.at[:, own_q], v_group),
    ]

    barrier = pltpu.get_barrier_semaphore()
    greeted = y_c + z_c[:] + x_only
    greeted = list(dict.fromkeys(greeted))
    for o in greeted:
        pl.semaphore_signal(barrier, inc=1, device_id=at(*o), device_id_type=MESH)

    for copy in ld_residual:
        copy.wait()
    normed = rms_scale(v_residual[...].astype(F32), v_norm_gain[...].astype(F32)).astype(BF16)
    for i in range(s.Z):
        normed_out[i] = normed[:, i * s.zb : (i + 1) * s.zb]
    for copy in ld_weights:
        copy.wait()

    pl.semaphore_wait(barrier, len(greeted))

    for o in y_c:
        to = at(*o)
        send(PROJ_W, w_own.at[to[2]], w_row.at[own_rows, :], to)
    for o in z_c:
        to = at(*o)
        send(PROJ_T, normed_out.at[to[0]], normed_in.at[z * s.C + c], to)
    for o in z_only:
        pl.semaphore_signal(plane_sem, inc=1, device_id=at(*o), device_id_type=MESH)
    ld_out_w[0].wait()
    for o in y_c:
        to = at(*o)
        send(OUT_W, out_w.at[own_rows, :], out_w.at[own_rows, :], to)
    for o in x_only:
        to = at(*o)
        their_q = pl.ds(pl.multiple_of(to[3] * s.dq, s.dq), s.dq)
        send(GATE_W, w_gate.at[their_q, :], gate_w.at[:, own_f], to)
        send(GATE_W, w_up.at[their_q, :], gate_w.at[:, own_f2], to)
    for o in x_only:
        to = at(*o)
        their_q = pl.ds(pl.multiple_of(to[3] * s.dq, s.dq), s.dq)
        send(DOWN_W, w_down.at[:, their_q], down_w.at[own_f, :], to)

    normed_in[z * s.C + c] = normed_out[z]
    w_row[own_rows, :] = w_own[c]

    ld_ids.wait()
    tokens = s.tokens
    ids = v_ids[...]
    first, second = ids[0:1], ids[1:2]
    partner_expert = plane * s.C + other_c
    own_named = ((first == expert) | (second == expert)).astype(F32)
    par_named = ((first == partner_expert) | (second == partner_expert)).astype(F32)
    named = jnp.concatenate([own_named, par_named, jnp.zeros((6, tokens), F32)], axis=0)
    t_row = lax.broadcasted_iota(jnp.int32, (tokens, tokens), 0)
    t_col = lax.broadcasted_iota(jnp.int32, (tokens, tokens), 1)
    upto = (t_row <= t_col).astype(BF16)
    code = named * matmul(named.astype(BF16), upto)
    slot_full = lax.broadcasted_iota(jnp.int32, (CAP, tokens), 0).astype(F32) + 1.0
    rival = jnp.where(first == expert, second, first).astype(F32)
    own_full = jnp.where(slot_full == code[0:1], 1.0, 0.0)
    rival_id = jnp.sum(own_full * rival, axis=1, keepdims=True).astype(jnp.int32)
    side = tokens // 2
    p_row = lax.broadcasted_iota(jnp.int32, (tokens, side), 0)
    p_col = lax.broadcasted_iota(jnp.int32, (tokens, side), 1)
    p_tok = 2 * p_col - lax.rem(p_col, 2)
    slot_side = lax.broadcasted_iota(jnp.int32, (CAP, side), 0).astype(F32) + 1.0
    code_c = matmul(code.astype(BF16), (p_row == p_tok + 2 * c).astype(BF16))
    code_o = matmul(code.astype(BF16), (p_row == p_tok + 2 * other_c).astype(BF16))
    own_here = (slot_side == code_c[0:1]).astype(F32)
    par_here = (slot_side == code_c[1:2]).astype(F32)
    own_there = (slot_side == code_o[0:1]).astype(F32)
    own_here_t = own_here.T.astype(BF16)
    own_there_t = own_there.T.astype(BF16)

    all_of(PROJ_T, normed_in.at[pl.ds(0, len(z_c))]).wait_recv()
    all_of(PROJ_W, w_row.at[pl.ds(0, len(y_c) * s.rows), :]).wait_recv()
    lines = s.Z * s.C
    sums = matmul(normed_in[...].reshape(2 * lines, s.zb), w_row[...])
    sums_out[...] = sums.astype(BF16).reshape(lines, 2, half_w)
    for o in z_c:
        to = at(*o)
        send(PROJ_SUM, sums_out.at[to[0] * s.C + to[2]], sums_in.at[c, z], to)
    sums_in[c, z] = sums_out[z * s.C + c]

    for copy in ld_state:
        copy.wait()
    all_of(PROJ_SUM, sums_out.at[pl.ds(0, len(z_c))]).wait_recv()
    low = jnp.sum(sums_in[0].astype(F32), axis=0)
    high = jnp.sum(sums_in[1].astype(F32), axis=0)
    query = low[:, :k].astype(BF16).astype(F32) * k ** (-0.5)
    key = low[:, k : 2 * k].astype(BF16).astype(F32)
    decay = jnp.concatenate([low[:, 2 * k :], high[:, : k // 2]], axis=1) + v_bias[...]
    value = high[:, k // 2 :].astype(BF16).astype(F32)
    log_decay = jnp.minimum(decay, 0.0) - jnp.log1p(jnp.exp(-jnp.abs(decay)))
    alpha = jnp.exp(log_decay / GATE_SCALE)
    query_alpha = jnp.concatenate([query * alpha, jnp.zeros((6, k), F32)], axis=0).T
    read_out = jnp.concatenate(
        [
            jnp.sum(query_alpha[:, 0:1] * v_state[0], axis=0, keepdims=True),
            jnp.sum(query_alpha[:, 1:2] * v_state[1], axis=0, keepdims=True),
        ],
        axis=0,
    )
    read_out = read_out + jnp.sum(query * key, axis=1, keepdims=True) * value
    heads[z] = rms_scale(read_out, v_head_gain[...].astype(F32)).astype(BF16)
    for o in z_only:
        send(HEADS, heads.at[z], heads.at[z], at(*o))
    v_alpha[...] = alpha
    v_key[...] = key
    v_value[...] = value
    stores = [
        pltpu.make_async_copy(v_alpha, alpha_out, store_sem.at[0]),
        pltpu.make_async_copy(v_key, key_out, store_sem.at[1]),
        pltpu.make_async_copy(v_value, value_out, store_sem.at[2]),
    ]
    for copy in stores:
        copy.start()

    pl.semaphore_wait(plane_sem, len(z_only))
    all_of(OUT_W, out_w.at[pl.ds(0, len(y_c) * s.rows), :]).wait_recv()
    all_of(HEADS, heads.at[pl.ds(0, len(z_only))]).wait_recv()
    part = matmul_t(heads[...].reshape(2 * s.Z, s.dvh), out_w[...])
    head_out[...] = part.astype(BF16).reshape(s.Z, 2, s.zb)
    for o in z_x:
        to = at(*o)
        send(HEAD_SUM, head_out.at[to[0]], head_in.at[z * s.X + x], to)
    head_in[z * s.X + x] = head_out[z]
    for copy in ld_ffn:
        copy.wait()
    all_of(HEAD_SUM, head_in.at[pl.ds(0, len(z_x))]).wait_recv()
    blocks = []
    for i in range(s.Z):
        total = head_in[i * s.X].astype(F32)
        for j in range(1, s.X):
            total = total + head_in[i * s.X + j].astype(F32)
        blocks.append(total)
    hidden_res = v_residual[...].astype(F32) + jnp.concatenate(blocks, axis=1)
    hidden_res = hidden_res.astype(BF16).astype(F32)
    moe_rows = rms_scale(hidden_res, v_ffn_gain[...].astype(F32)).astype(BF16)
    for i in range(s.X):
        moe_in[i] = moe_rows[:, i * s.dq : (i + 1) * s.dq]
        hidden_q[i] = hidden_res[:, i * s.dq : (i + 1) * s.dq]

    gathered[plane] = moe_in[x]
    for o in z_y:
        send(GATHER, moe_in.at[x], gathered.at[plane], at(*o))
    for copy in ld_moe:
        copy.wait()
    all_of(GATHER, gathered.at[pl.ds(0, len(z_y))]).wait_recv()
    rows = gathered[...].reshape(side, s.dq)
    picked_out[...] = matmul(par_here.astype(BF16), rows).astype(BF16)
    send(PICKED, picked_out, picked_in, partner)
    picked = matmul(own_here.astype(BF16), rows)
    all_of(GATE_W, gate_w.at[:, pl.ds(0, 2 * len(x_only) * s.fh)]).wait_recv()
    all_of(PICKED, picked_in).wait_recv()
    picked = (picked + picked_in[...].astype(F32)).astype(BF16)
    wide = 2 * s.ff
    partial[x, :, 0:wide] = matmul(picked, gate_w[...]).astype(BF16)
    partial[x, :, wide : wide + s.experts] = matmul_t(picked, v_router[...]).astype(BF16)
    groups = matmul_t(picked, v_group[...]).astype(BF16)
    partial[x, :, wide + s.experts : wide + s.experts + s.groups] = groups
    for o in x_only:
        send(GATE_SUM, partial.at[x], partial.at[x], at(*o))
    all_of(DOWN_W, down_w.at[pl.ds(0, len(x_only) * s.fh), :]).wait_recv()
    all_of(GATE_SUM, partial.at[pl.ds(0, len(x_only))]).wait_recv()
    both = jnp.sum(partial[:, :, 0:wide].astype(F32), axis=0)
    gate, up = both[:, : s.ff], both[:, s.ff :]
    hidden = (gate * (1.0 / (1.0 + jnp.exp(-gate))) * up).astype(BF16)
    output = matmul(hidden, down_w[...])
    logits = jnp.sum(partial[:, :, wide : wide + s.experts].astype(F32), axis=0)
    groups = jnp.sum(
        partial[:, :, wide + s.experts : wide + s.experts + s.groups].astype(F32), axis=0
    )
    lane = lax.broadcasted_iota(jnp.int32, logits.shape, 1)
    chosen = jnp.sum(jnp.where(lane == expert, logits, 0.0), axis=1, keepdims=True)
    against = jnp.sum(jnp.where(lane == rival_id, logits, 0.0), axis=1, keepdims=True)
    g_lane = lax.broadcasted_iota(jnp.int32, groups.shape, 1)
    own_group = lax.div(expert, s.experts // s.groups)
    g_own = jnp.sum(jnp.where(g_lane == own_group, groups, 0.0), axis=1, keepdims=True)
    share = 1.0 / jnp.sum(jnp.exp(groups - g_own), axis=1, keepdims=True)
    weight = share * (1.0 / (1.0 + jnp.exp(against - chosen)))
    scaled = (output * weight).astype(BF16)

    merge_out[...] = matmul(own_there_t, scaled).astype(BF16)
    send(MERGE, merge_out, merge_in, partner)
    here = matmul(own_here_t, scaled)
    all_of(MERGE, merge_in).wait_recv()
    merged = (here + merge_in[...].astype(F32)).astype(BF16)
    combine_out[...] = merged.reshape(side // 2, 2, s.dq)
    for o in z_y:
        to = at(*o)
        send(COMBINE, combine_out.at[to[0] * s.Y + to[1]], combine_in.at[plane], to)
    combine_in[plane] = combine_out[plane]
    all_of(COMBINE, combine_in.at[pl.ds(0, len(z_y))]).wait_recv()
    moe_sum = jnp.sum(combine_in[...].astype(F32), axis=0)
    quarters[x] = (hidden_q[x] + moe_sum).astype(BF16)
    for o in x_only:
        send(QUARTERS, quarters.at[x], quarters.at[x], at(*o))
    all_of(QUARTERS, quarters.at[pl.ds(0, len(x_only))]).wait_recv()
    for i in range(s.X):
        v_layer[:, i * s.dq : (i + 1) * s.dq] = quarters[i]
    done = pltpu.make_async_copy(v_layer, layer_out, store_sem.at[3])
    done.start()

    all_of(PROJ_W, w_row.at[pl.ds(0, len(y_c) * s.rows), :]).wait_send()
    all_of(PROJ_T, normed_in.at[pl.ds(0, len(z_c))]).wait_send()
    all_of(OUT_W, out_w.at[pl.ds(0, len(y_c) * s.rows), :]).wait_send()
    all_of(PROJ_SUM, sums_out.at[pl.ds(0, len(z_c))]).wait_send()
    all_of(HEADS, heads.at[pl.ds(0, len(z_only))]).wait_send()
    all_of(HEAD_SUM, head_in.at[pl.ds(0, len(z_x))]).wait_send()
    all_of(GATHER, gathered.at[pl.ds(0, len(z_y))]).wait_send()
    all_of(PICKED, picked_out).wait_send()
    all_of(GATE_W, gate_w.at[:, pl.ds(0, 2 * len(x_only) * s.fh)]).wait_send()
    all_of(DOWN_W, down_w.at[pl.ds(0, len(x_only) * s.fh), :]).wait_send()
    all_of(GATE_SUM, partial.at[pl.ds(0, len(x_only))]).wait_send()
    all_of(MERGE, merge_out).wait_send()
    all_of(COMBINE, combine_in.at[pl.ds(0, len(z_y))]).wait_send()
    all_of(QUARTERS, quarters.at[pl.ds(0, len(x_only))]).wait_send()
    for copy in stores:
        copy.wait()
    done.wait()


def on_device(
    s,
    residual_in,
    gla_state,
    norm_gain,
    w_query,
    w_key,
    w_value,
    w_decay,
    decay_bias,
    head_gain,
    w_output,
    ffn_gain,
    router_group,
    router_expert,
    expert_ids,
    w_gate,
    w_up,
    w_down,
):
    old_state = gla_state[:, 0]
    side = s.tokens // 2
    vmem = pltpu.VMEM
    scratch = [
        vmem((2, s.d), BF16),
        vmem((1, s.d), BF16),
        vmem((1, s.dkh), F32),
        vmem((1, s.dvh), BF16),
        vmem((1, s.d), BF16),
        vmem((2, s.tokens), jnp.int32),
        vmem((2, s.dkh, s.dvh), F32),
        vmem((s.experts, s.dq), BF16),
        vmem((s.groups, s.dq), BF16),
        vmem((2, s.rows, s.half), BF16),
        vmem((s.zb, s.half), BF16),
        vmem((s.Z, 2, s.zb), BF16),
        vmem((s.Z * s.C, 2, s.zb), BF16),
        vmem((s.zb, s.dvh), BF16),
        vmem((s.Z * s.C, 2, s.half), BF16),
        vmem((2, s.Z, 2, s.half), BF16),
        vmem((s.Z, 2, s.dvh), BF16),
        vmem((s.Z, 2, s.zb), BF16),
        vmem((s.Z * s.X, 2, s.zb), BF16),
        vmem((s.X, 2, s.dq), BF16),
        vmem((s.X, 2, s.dq), F32),
        vmem((side // 2, 2, s.dq), BF16),
        vmem((CAP, s.dq), BF16),
        vmem((CAP, s.dq), BF16),
        vmem((s.dq, 2 * s.ff), BF16),
        vmem((s.ff, s.dq), BF16),
        vmem((s.X, CAP, 2 * s.ff + s.experts + 128), BF16),
        vmem((side, s.dq), BF16),
        vmem((side, s.dq), BF16),
        vmem((side // 2, 2, s.dq), BF16),
        vmem((side // 2, 2, s.dq), BF16),
        vmem((s.X, 2, s.dq), BF16),
        vmem((2, s.dkh), F32),
        vmem((2, s.dkh), F32),
        vmem((2, s.dvh), F32),
        vmem((2, s.d), BF16),
        pltpu.SemaphoreType.DMA((18,)),
        pltpu.SemaphoreType.DMA((4,)),
        pltpu.SemaphoreType.DMA((EXCHANGES,)),
        pltpu.SemaphoreType.DMA((EXCHANGES,)),
        pltpu.SemaphoreType.REGULAR,
    ]
    args = (
        residual_in,
        norm_gain[None],
        w_query,
        w_key,
        w_value,
        w_decay,
        decay_bias[None],
        old_state,
        head_gain[None],
        w_output.T,
        ffn_gain[None],
        router_group.T,
        router_expert,
        expert_ids.T,
        w_gate[0],
        w_up[0],
        w_down[0],
    )
    anywhere = pl.BlockSpec(memory_space=pl.ANY)
    layer_out, alpha, key, value = pl.pallas_call(
        functools.partial(layer_kernel, s),
        out_shape=(
            jax.ShapeDtypeStruct((2, s.d), BF16),
            jax.ShapeDtypeStruct((2, s.dkh), F32),
            jax.ShapeDtypeStruct((2, s.dkh), F32),
            jax.ShapeDtypeStruct((2, s.dvh), F32),
        ),
        in_specs=[anywhere] * len(args),
        out_specs=(anywhere,) * 4,
        scratch_shapes=scratch,
        compiler_params=pltpu.CompilerParams(collective_id=0, has_side_effects=True),
        name="layer",
    )(*args)
    new_state = alpha[:, :, None] * old_state + key[:, :, None] * value[:, None, :]
    return layer_out, new_state[:, None]


def build(torus, residual, state, w_gate, router_group):
    Z, Y, C, X = (torus.shape[a] for a in AXES)
    tokens, d = residual
    experts, _, ff = w_gate
    dkh, dvh = state[2], state[3]
    s = types.SimpleNamespace(
        Z=Z,
        Y=Y,
        C=C,
        X=X,
        tokens=tokens,
        d=d,
        rows=d // (Z * Y * C),
        zb=d // Z,
        dq=d // X,
        dkh=dkh,
        dvh=dvh,
        half=(3 * dkh + dvh) // 2,
        ff=ff,
        fh=ff // X,
        experts=experts,
        groups=router_group[1],
    )
    in_specs = (
        P(EP, None),
        P(EP, "x", None, None),
        P(),
        P(EP, "x"),
        P(EP, "x"),
        P(EP, "x"),
        P(EP, "x"),
        P("x"),
        P(),
        P("x", EP),
        P(),
        P(),
        P(),
        P(),
        P(EP, None, "x"),
        P(EP, None, "x"),
        P(EP, "x", None),
    )
    out_specs = (P(EP, None), P(EP, "x", None, None))
    return jax.shard_map(
        functools.partial(on_device, s),
        mesh=torus,
        in_specs=in_specs,
        out_specs=out_specs,
        check_vma=False,
    )


def solution(mesh):
    torus = Mesh(mesh.devices.reshape(8, 8, 2, mesh.shape["tp"]), AXES)

    def layer(*args):
        shapes = args[0].shape, args[1].shape, args[14].shape, args[11].shape
        return build(torus, *shapes)(*args)

    return layer
```

time: 203 us -> 73.7 us (0.36)
  waiting for transfers between devices: 84.1 us -> 0 us
  Pallas kernels: 0 us -> 67.1 us
  blocking collectives: 50.2 us -> 0 us
  starting transfers between devices: 39.4 us -> 0 us
  local copies, waits for them, and re-layouts: 12.6 us -> 3.81 us
  matrix products: 6.88 us -> 0 us
  other arithmetic: 7.32 us -> 1.85 us
    all_to_all x8 -> x0, waiting for transfers between devices: 84.1 us -> none  [the longest x4 33.2 us: from_everyone(): return lax.all_to_all(copies, axis, split_axis=0, concat_axis=0, tiled=True)]
    pallas_call x0 -> x1, Pallas kernels: none -> 67.1 us  [on_device(): pl.pallas_call(functools.partial(layer_kernel, s), out_shape=(jax.ShapeDt...]
    all_to_all x4 -> x0, blocking collectives: 50.2 us -> none  [the longest x1 29.7 us: on_device(): lax.all_to_all(normed, EP, split_axis=1, concat_axis=0, tiled=True)]
    all_to_all x8 -> x0, starting transfers between devices: 39.4 us -> none  [the longest x4 19 us: from_everyone(): return lax.all_to_all(copies, axis, split_axis=0, concat_axis=0, tiled=True)]
    dot_general x12 -> x0, matrix products: 6.88 us -> none  [the longest x1 1.39 us: on_device(): output = jnp.dot(hidden, w_down[0], preferred_element_type=jnp.float32)]
    reduce_sum x10 -> x0, other arithmetic: 3.82 us -> none  [the longest x1 2.04 us: summed_on_arrival(): return arrived.sum(axis=0)]
    another operation x5 -> x0, local copies, waits for them, and re-layouts: 2.57 us -> none  [the longest x2 1.57 us: in_order(): return jnp.moveaxis(blocks, 0, dim).reshape(shape)]
    transpose x2 -> x0, local copies, waits for them, and re-layouts: 2.38 us -> none  [whole_of(): return in_order(blocks.swapaxes(0, 1).reshape(-1, *shard.shape), dim)]
  transfers between devices with their start and end apart: 8 -> 0, of which waited for: 8 -> 0; matrix products, arithmetic and copies ran while one was open for 1% -> 0% of each run, Pallas kernels for 0% -> 0%
where the time goes in v1:
time: 73.7 us; the launch traced here: 73.4 us
  Pallas kernels  67.1 us (91%)
  local copies, waits for them, and re-layouts  3.81 us (5%)
  other arithmetic  1.85 us (3%)
    pallas_call x1, Pallas kernels, on_device(): pl.pallas_call(functools.partial(layer_kernel, s), out_shape=(jax.ShapeDt...  67.1 us
    unnamed x15, local copies, waits for them, and re-layouts  2.04 us
    add x1, other arithmetic, on_device(): alpha[:, :, None] * old_state + key[:, :, None] * value[:, None, :]  1.85 us

profile of v1, /device:TPU:1, one launch (start us, length us, event | category | flops | bytes accessed | tf_op | source)
XLA Modules:
  0.0 73.4 jit_solution(2342120519186484157)
XLA Ops:
  0.6 0.0 copy-start.3
  0.6 0.0 copy-start.6
  0.6 0.7 copy-done.6
  1.3 0.6 broadcast_in_dim.18.head_gain
  1.9 0.0 copy-done.3
  1.9 0.0 copy-start.4
  1.9 0.6 broadcast_in_dim.16.norm_gain
  2.5 0.1 copy-done.4
  2.6 0.6 broadcast_in_dim.19.ffn_gain
  3.2 0.0 copy-start
  3.2 67.1 %layer.1 = (bf16[2,2048]{1,0:T(2,128)(2,1)}, f32[2,256]{1,0:T(2,128)}, f32[2,256]{1,0:T(2,128)}, f32[2,512]{1,0:T(2,128)}) custom-call(bf16[2,2048]{1,0:T(2,128)(2,1)} %residual.1, bf16[1,2048]{1,0:T(2,128)(2,1)} %broadcast_in_dim.16.norm_gain, bf16[16,256]{1,0:T(8,128)(2,1)} %w_query.1, bf16[16,256]{1,0:T(8,128)(2,1)} %w_key.1, bf16[16,512]{1,0:T(8,128)(2,1)} %w_value.1, ...), custom_call_target="tpu_custom_call" | custom-call | tf_op jit(solution)/shard_map/layer/pallas_call | solution.py:509
  70.3 0.0 copy-start.2
  70.3 0.0 copy-start.5
  70.3 0.0 copy-done
  70.3 0.7 copy-done.2
  70.9 0.0 copy-done.5
  71.0 0.0 copy-start.1
  71.0 1.9 %multiply_add_fusion = f32[2,1,256,512]{3,2,1,0:T(8,128)} fusion(f32[2,1,256,512]{3,2,1,0:T(8,128)S(1)} %copy-done, f32[2,512]{1,0:T(2,128)S(1)} %copy-done.2, f32[2,256]{1,0:T(2,128)} %get-tuple-element.8, f32[2,256]{1,0:T(2,128)S(1)} %copy-done.5), kind=kLoop, calls=%fused_computation | loop fusion | flops 786432 | bytes 2105344 | tf_op jit(solution)/shard_map/add | solution.py:523
  72.8 0.0 copy-done.1
  72.8 0.6 copy.20
Async XLA Ops:
  0.6 1.3 %copy-start.3 = (bf16[2048]{0:T(1024)(128)(2,1)S(1)}, bf16[2048]{0:T(1024)(128)(2,1)}, u32[]{:S(2)}) copy-start(bf16[2048]{0:T(1024)(128)(2,1)} %param.19) | copy-start | bytes 12292
  0.6 0.7 copy-start.6
  1.9 0.7 copy-start.4
  3.2 67.1 %copy-start = (f32[2,1,256,512]{3,2,1,0:T(8,128)S(1)}, f32[2,1,256,512]{3,2,1,0:T(8,128)}, u32[]{:S(2)}) copy-start(f32[2,1,256,512]{3,2,1,0:T(8,128)} %param.18) | copy-start | bytes 3145732
  70.3 0.7 copy-start.2
  70.3 0.7 copy-start.5
  71.0 1.9 %copy-start.1 = (bf16[2,2048]{1,0:T(2,128)(2,1)S(1)}, bf16[2,2048]{1,0:T(2,128)(2,1)}, u32[]{:S(2)}) copy-start(bf16[2,2048]{1,0:T(2,128)(2,1)} %get-tuple-element.12) | copy-start | bytes 24580

commit v2 on v1

--- a/solution.py
+++ b/solution.py
@@ -52,6 +52,21 @@
 
 def matmul_t(a, b):
     return lax.dot_general(a, b, (((1,), (1,)), ((), ())), preferred_element_type=F32)
+
+
+def row_of(ref):
+    return ref[...].astype(F32).reshape(1, ref.shape[0])
+
+
+def store_kernel(layer, state, layer_out, state_out, sem):
+    copies = [
+        pltpu.make_async_copy(layer, layer_out, sem.at[0]),
+        pltpu.make_async_copy(state, state_out, sem.at[1]),
+    ]
+    for copy in copies:
+        copy.start()
+    for copy in copies:
+        copy.wait()
 
 
 def layer_kernel(
@@ -74,9 +89,7 @@
     w_up,
     w_down,
     layer_out,
-    alpha_out,
-    key_out,
-    value_out,
+    new_state,
     v_residual,
     v_norm_gain,
     v_bias,
@@ -109,12 +122,7 @@
     combine_out,
     combine_in,
     quarters,
-    v_alpha,
-    v_key,
-    v_value,
-    v_layer,
     load_sem,
-    store_sem,
     send_sem,
     recv_sem,
     plane_sem,
@@ -126,21 +134,25 @@
     expert = plane * s.C + c
     half_w = s.half
 
-    def at(dz=0, dy=0, dc=0, dx=0):
+    pair = lax.rem(y, 2)
+    line = (z * 2 + pair) * s.C + c
+
+    def at(dz=0, dy=0, dc=0, dx=0, across=0):
         return (
             lax.rem(z + dz, s.Z) if dz else z,
-            lax.rem(y + dy, s.Y) if dy else y,
+            y + 1 - 2 * pair if across else lax.rem(y + dy, s.Y) if dy else y,
             lax.rem(c + dc, s.C) if dc else c,
             lax.rem(x + dx, s.X) if dx else x,
         )
 
     def ordered(offsets):
         def far(o):
-            return -(rounds(s.Z, o[0]) + rounds(s.Y, o[1]) + rounds(s.X, o[3]))
+            return -(rounds(s.Z, o[0]) + rounds(s.Y, o[1]) + rounds(s.X, o[3]) + sum(o[4:]))
 
         return sorted((o for o in offsets if any(o)), key=far)
 
-    z_c = ordered((i, 0, k, 0) for i in range(s.Z) for k in range(s.C))
+    z_p = ordered((i, 0, k, 0, p) for i in range(s.Z) for k in range(s.C) for p in range(2))
+    y_w = ordered((0, i, k, 0) for i in range(0, s.Y, 2) for k in range(s.C))
     y_c = ordered((0, i, k, 0) for i in range(s.Y) for k in range(s.C))
     z_only = ordered((i, 0, 0, 0) for i in range(s.Z))
     z_x = ordered((i, 0, 0, j) for i in range(s.Z) for j in range(s.X))
@@ -191,6 +203,7 @@
     own_f = pl.ds(pl.multiple_of(x * s.fh, s.fh), s.fh)
     own_f2 = pl.ds(pl.multiple_of(s.ff + x * s.fh, s.fh), s.fh)
     ld_state = [load(decay_bias, v_bias), load(head_gain, v_head_gain), load(state, v_state)]
+    w_row[...] = jnp.zeros_like(w_row)
     ld_out_w = [load(w_output_t, out_w.at[own_rows, :])]
     ld_ffn = [load(ffn_gain, v_ffn_gain)]
     ld_moe = [
@@ -202,27 +215,26 @@
     ]
 
     barrier = pltpu.get_barrier_semaphore()
-    greeted = y_c + z_c[:] + x_only
-    greeted = list(dict.fromkeys(greeted))
+    greeted = y_c + [o for o in z_p if o[0]] + x_only
     for o in greeted:
         pl.semaphore_signal(barrier, inc=1, device_id=at(*o), device_id_type=MESH)
 
+    for copy in ld_weights:
+        copy.wait()
+
+    pl.semaphore_wait(barrier, len(greeted))
+
+    for o in y_w:
+        to = at(*o)
+        send(PROJ_W, w_own.at[to[2]], w_row.at[own_rows, :], to)
     for copy in ld_residual:
         copy.wait()
-    normed = rms_scale(v_residual[...].astype(F32), v_norm_gain[...].astype(F32)).astype(BF16)
+    normed = rms_scale(v_residual[...].astype(F32), row_of(v_norm_gain)).astype(BF16)
     for i in range(s.Z):
         normed_out[i] = normed[:, i * s.zb : (i + 1) * s.zb]
-    for copy in ld_weights:
-        copy.wait()
-
-    pl.semaphore_wait(barrier, len(greeted))
-
-    for o in y_c:
-        to = at(*o)
-        send(PROJ_W, w_own.at[to[2]], w_row.at[own_rows, :], to)
-    for o in z_c:
-        to = at(*o)
-        send(PROJ_T, normed_out.at[to[0]], normed_in.at[z * s.C + c], to)
+    for o in z_p:
+        to = at(*o)
+        send(PROJ_T, normed_out.at[to[0]], normed_in.at[line], to)
     for o in z_only:
         pl.semaphore_signal(plane_sem, inc=1, device_id=at(*o), device_id_type=MESH)
     ld_out_w[0].wait()
@@ -239,7 +251,7 @@
         their_q = pl.ds(pl.multiple_of(to[3] * s.dq, s.dq), s.dq)
         send(DOWN_W, w_down.at[:, their_q], down_w.at[own_f, :], to)
 
-    normed_in[z * s.C + c] = normed_out[z]
+    normed_in[line] = normed_out[z]
     w_row[own_rows, :] = w_own[c]
 
     ld_ids.wait()
@@ -271,49 +283,43 @@
     own_here_t = own_here.T.astype(BF16)
     own_there_t = own_there.T.astype(BF16)
 
-    all_of(PROJ_T, normed_in.at[pl.ds(0, len(z_c))]).wait_recv()
-    all_of(PROJ_W, w_row.at[pl.ds(0, len(y_c) * s.rows), :]).wait_recv()
-    lines = s.Z * s.C
+    all_of(PROJ_T, normed_in.at[pl.ds(0, len(z_p))]).wait_recv()
+    all_of(PROJ_W, w_row.at[pl.ds(0, len(y_w) * s.rows), :]).wait_recv()
+    lines = s.Z * 2 * s.C
     sums = matmul(normed_in[...].reshape(2 * lines, s.zb), w_row[...])
     sums_out[...] = sums.astype(BF16).reshape(lines, 2, half_w)
-    for o in z_c:
-        to = at(*o)
-        send(PROJ_SUM, sums_out.at[to[0] * s.C + to[2]], sums_in.at[c, z], to)
-    sums_in[c, z] = sums_out[z * s.C + c]
+    for o in z_p:
+        to = at(*o)
+        to_line = (to[0] * 2 + lax.rem(to[1], 2)) * s.C + to[2]
+        send(PROJ_SUM, sums_out.at[to_line], sums_in.at[c, z * 2 + pair], to)
+    sums_in[c, z * 2 + pair] = sums_out[line]
 
     for copy in ld_state:
         copy.wait()
-    all_of(PROJ_SUM, sums_out.at[pl.ds(0, len(z_c))]).wait_recv()
+    all_of(PROJ_SUM, sums_out.at[pl.ds(0, len(z_p))]).wait_recv()
     low = jnp.sum(sums_in[0].astype(F32), axis=0)
     high = jnp.sum(sums_in[1].astype(F32), axis=0)
     query = low[:, :k].astype(BF16).astype(F32) * k ** (-0.5)
     key = low[:, k : 2 * k].astype(BF16).astype(F32)
-    decay = jnp.concatenate([low[:, 2 * k :], high[:, : k // 2]], axis=1) + v_bias[...]
+    decay = jnp.concatenate([low[:, 2 * k :], high[:, : k // 2]], axis=1) + row_of(v_bias)
     value = high[:, k // 2 :].astype(BF16).astype(F32)
     log_decay = jnp.minimum(decay, 0.0) - jnp.log1p(jnp.exp(-jnp.abs(decay)))
     alpha = jnp.exp(log_decay / GATE_SCALE)
-    query_alpha = jnp.concatenate([query * alpha, jnp.zeros((6, k), F32)], axis=0).T
+    factors = jnp.concatenate([query * alpha, alpha, key, jnp.zeros((2, k), F32)], axis=0).T
     read_out = jnp.concatenate(
         [
-            jnp.sum(query_alpha[:, 0:1] * v_state[0], axis=0, keepdims=True),
-            jnp.sum(query_alpha[:, 1:2] * v_state[1], axis=0, keepdims=True),
+            jnp.sum(factors[:, 0:1] * v_state[0], axis=0, keepdims=True),
+            jnp.sum(factors[:, 1:2] * v_state[1], axis=0, keepdims=True),
         ],
         axis=0,
     )
     read_out = read_out + jnp.sum(query * key, axis=1, keepdims=True) * value
-    heads[z] = rms_scale(read_out, v_head_gain[...].astype(F32)).astype(BF16)
+    heads[z] = rms_scale(read_out, row_of(v_head_gain)).astype(BF16)
     for o in z_only:
         send(HEADS, heads.at[z], heads.at[z], at(*o))
-    v_alpha[...] = alpha
-    v_key[...] = key
-    v_value[...] = value
-    stores = [
-        pltpu.make_async_copy(v_alpha, alpha_out, store_sem.at[0]),
-        pltpu.make_async_copy(v_key, key_out, store_sem.at[1]),
-        pltpu.make_async_copy(v_value, value_out, store_sem.at[2]),
-    ]
-    for copy in stores:
-        copy.start()
+    for i in range(2):
+        carried = factors[:, 2 + i : 3 + i] * v_state[i]
+        new_state[i] = carried + factors[:, 4 + i : 5 + i] * value[i : i + 1]
 
     pl.semaphore_wait(plane_sem, len(z_only))
     all_of(OUT_W, out_w.at[pl.ds(0, len(y_c) * s.rows), :]).wait_recv()
@@ -335,7 +341,7 @@
         blocks.append(total)
     hidden_res = v_residual[...].astype(F32) + jnp.concatenate(blocks, axis=1)
     hidden_res = hidden_res.astype(BF16).astype(F32)
-    moe_rows = rms_scale(hidden_res, v_ffn_gain[...].astype(F32)).astype(BF16)
+    moe_rows = rms_scale(hidden_res, row_of(v_ffn_gain)).astype(BF16)
     for i in range(s.X):
         moe_in[i] = moe_rows[:, i * s.dq : (i + 1) * s.dq]
         hidden_q[i] = hidden_res[:, i * s.dq : (i + 1) * s.dq]
@@ -397,14 +403,12 @@
         send(QUARTERS, quarters.at[x], quarters.at[x], at(*o))
     all_of(QUARTERS, quarters.at[pl.ds(0, len(x_only))]).wait_recv()
     for i in range(s.X):
-        v_layer[:, i * s.dq : (i + 1) * s.dq] = quarters[i]
-    done = pltpu.make_async_copy(v_layer, layer_out, store_sem.at[3])
-    done.start()
-
-    all_of(PROJ_W, w_row.at[pl.ds(0, len(y_c) * s.rows), :]).wait_send()
-    all_of(PROJ_T, normed_in.at[pl.ds(0, len(z_c))]).wait_send()
+        layer_out[:, i * s.dq : (i + 1) * s.dq] = quarters[i]
+
+    all_of(PROJ_W, w_row.at[pl.ds(0, len(y_w) * s.rows), :]).wait_send()
+    all_of(PROJ_T, normed_in.at[pl.ds(0, len(z_p))]).wait_send()
     all_of(OUT_W, out_w.at[pl.ds(0, len(y_c) * s.rows), :]).wait_send()
-    all_of(PROJ_SUM, sums_out.at[pl.ds(0, len(z_c))]).wait_send()
+    all_of(PROJ_SUM, sums_out.at[pl.ds(0, len(z_p))]).wait_send()
     all_of(HEADS, heads.at[pl.ds(0, len(z_only))]).wait_send()
     all_of(HEAD_SUM, head_in.at[pl.ds(0, len(z_x))]).wait_send()
     all_of(GATHER, gathered.at[pl.ds(0, len(z_y))]).wait_send()
@@ -415,9 +419,6 @@
     all_of(MERGE, merge_out).wait_send()
     all_of(COMBINE, combine_in.at[pl.ds(0, len(z_y))]).wait_send()
     all_of(QUARTERS, quarters.at[pl.ds(0, len(x_only))]).wait_send()
-    for copy in stores:
-        copy.wait()
-    done.wait()
 
 
 def on_device(
@@ -445,10 +446,10 @@
     vmem = pltpu.VMEM
     scratch = [
         vmem((2, s.d), BF16),
-        vmem((1, s.d), BF16),
-        vmem((1, s.dkh), F32),
-        vmem((1, s.dvh), BF16),
-        vmem((1, s.d), BF16),
+        vmem((s.d,), BF16),
+        vmem((s.dkh,), F32),
+        vmem((s.dvh,), BF16),
+        vmem((s.d,), BF16),
         vmem((2, s.tokens), jnp.int32),
         vmem((2, s.dkh, s.dvh), F32),
         vmem((s.experts, s.dq), BF16),
@@ -456,10 +457,10 @@
         vmem((2, s.rows, s.half), BF16),
         vmem((s.zb, s.half), BF16),
         vmem((s.Z, 2, s.zb), BF16),
-        vmem((s.Z * s.C, 2, s.zb), BF16),
+        vmem((s.Z * 2 * s.C, 2, s.zb), BF16),
         vmem((s.zb, s.dvh), BF16),
-        vmem((s.Z * s.C, 2, s.half), BF16),
-        vmem((2, s.Z, 2, s.half), BF16),
+        vmem((s.Z * 2 * s.C, 2, s.half), BF16),
+        vmem((2, s.Z * 2, 2, s.half), BF16),
         vmem((s.Z, 2, s.dvh), BF16),
         vmem((s.Z, 2, s.zb), BF16),
         vmem((s.Z * s.X, 2, s.zb), BF16),
@@ -476,28 +477,23 @@
         vmem((side // 2, 2, s.dq), BF16),
         vmem((side // 2, 2, s.dq), BF16),
         vmem((s.X, 2, s.dq), BF16),
-        vmem((2, s.dkh), F32),
-        vmem((2, s.dkh), F32),
-        vmem((2, s.dvh), F32),
-        vmem((2, s.d), BF16),
         pltpu.SemaphoreType.DMA((18,)),
-        pltpu.SemaphoreType.DMA((4,)),
         pltpu.SemaphoreType.DMA((EXCHANGES,)),
         pltpu.SemaphoreType.DMA((EXCHANGES,)),
         pltpu.SemaphoreType.REGULAR,
     ]
     args = (
         residual_in,
-        norm_gain[None],
+        norm_gain,
         w_query,
         w_key,
         w_value,
         w_decay,
-        decay_bias[None],
+        decay_bias,
         old_state,
-        head_gain[None],
+        head_gain,
         w_output.T,
-        ffn_gain[None],
+        ffn_gain,
         router_group.T,
         router_expert,
         expert_ids.T,
@@ -506,21 +502,28 @@
         w_down[0],
     )
     anywhere = pl.BlockSpec(memory_space=pl.ANY)
-    layer_out, alpha, key, value = pl.pallas_call(
+    layer_out, new_state = pl.pallas_call(
         functools.partial(layer_kernel, s),
-        out_shape=(
-            jax.ShapeDtypeStruct((2, s.d), BF16),
-            jax.ShapeDtypeStruct((2, s.dkh), F32),
-            jax.ShapeDtypeStruct((2, s.dkh), F32),
-            jax.ShapeDtypeStruct((2, s.dvh), F32),
-        ),
+        out_shape=(pltpu.VMEM((2, s.d), BF16), pltpu.VMEM((2, s.dkh, s.dvh), F32)),
         in_specs=[anywhere] * len(args),
-        out_specs=(anywhere,) * 4,
+        out_specs=(pl.BlockSpec(memory_space=vmem),) * 2,
         scratch_shapes=scratch,
         compiler_params=pltpu.CompilerParams(collective_id=0, has_side_effects=True),
         name="layer",
     )(*args)
-    new_state = alpha[:, :, None] * old_state + key[:, :, None] * value[:, None, :]
+    held = [pltpu.with_memory_space_constraint(a, vmem) for a in (layer_out, new_state)]
+    layer_out, new_state = pl.pallas_call(
+        store_kernel,
+        out_shape=(
+            jax.ShapeDtypeStruct((2, s.d), BF16),
+            jax.ShapeDtypeStruct((2, s.dkh, s.dvh), F32),
+        ),
+        in_specs=[pl.BlockSpec(memory_space=vmem)] * 2,
+        out_specs=(anywhere,) * 2,
+        scratch_shapes=[pltpu.SemaphoreType.DMA((2,))],
+        compiler_params=pltpu.CompilerParams(vmem_limit_bytes=1 << 20),
+        name="store",
+    )(*held)
     return layer_out, new_state[:, None]
 
 

time: 73.7 us -> 66.7 us (0.905)
  local copies, waits for them, and re-layouts: 3.81 us -> 0 us
  other arithmetic: 1.85 us -> 0 us
  Pallas kernels: 67.1 us -> 65.9 us
    unnamed x15 -> x0, local copies, waits for them, and re-layouts: 2.04 us -> none
    add x1 -> x0, other arithmetic: 1.85 us -> none  [on_device(): alpha[:, :, None] * old_state + key[:, :, None] * value[:, None, :]]
    broadcast_in_dim x3 -> x0, local copies, waits for them, and re-layouts: 1.77 us -> none  [the longest x1 0.6 us: on_device(): norm_gain[None]]
    pallas_call x1 -> x2, Pallas kernels: 67.1 us -> 65.9 us  [the longest x1 64.9 us: on_device(): pl.pallas_call(functools.partial(layer_kernel, s), out_shape=(pltpu.VMEM(...]
where the time goes in v2:
time: 66.7 us; the launch traced here: 66.5 us
  Pallas kernels  65.9 us (99%)
    pallas_call x1, Pallas kernels, on_device(): pl.pallas_call(functools.partial(layer_kernel, s), out_shape=(pltpu.VMEM(...  64.9 us

profile of v2, /device:TPU:1, one launch (start us, length us, event | category | flops | bytes accessed | tf_op | source)
XLA Modules:
  0.0 66.5 jit_solution(4896360901297762416)
XLA Ops:
  0.6 64.9 %layer.1 = (bf16[2,2048]{1,0:T(2,128)(2,1)S(1)}, f32[2,256,512]{2,1,0:T(8,128)S(1)}) custom-call(bf16[2,2048]{1,0:T(2,128)(2,1)} %residual.1, bf16[2048]{0:T(1024)(128)(2,1)} %norm_gain.1, bf16[16,256]{1,0:T(8,128)(2,1)} %w_query.1, bf16[16,256]{1,0:T(8,128)(2,1)} %w_key.1, bf16[16,512]{1,0:T(8,128)(2,1)} %w_value.1, bf16[16,256]{1,0:T(8,128)(2,1)} %w_decay.1, ...), custom_call_target="tpu_custom_call" | custom-call | tf_op jit(solution)/shard_map/layer/pallas_call | solution.py:505
  65.5 1.0 %store.1 = (bf16[2,2048]{1,0:T(2,128)(2,1)}, f32[2,256,512]{2,1,0:T(8,128)}) custom-call(bf16[2,2048]{1,0:T(2,128)(2,1)S(1)} %get-tuple-element.6.layer, f32[2,256,512]{2,1,0:T(8,128)S(1)} %get-tuple-element.7.state), custom_call_target="tpu_custom_call" | custom-call | tf_op jit(solution)/shard_map/store/pallas_call | solution.py:515

commit v3 on v2

--- a/solution.py
+++ b/solution.py
@@ -21,7 +21,9 @@
 (
     PROJ_W,
     PROJ_T,
+    RESIDUAL,
     OUT_W,
+    OUT_PAIR,
     PROJ_SUM,
     HEADS,
     HEAD_SUM,
@@ -34,7 +36,7 @@
     COMBINE,
     QUARTERS,
     EXCHANGES,
-) = range(15)
+) = range(17)
 
 
 def rounds(n, offset):
@@ -109,8 +111,7 @@
     heads,
     head_out,
     head_in,
-    moe_in,
-    hidden_q,
+    residual_in,
     gathered,
     picked_out,
     picked_in,
@@ -137,9 +138,12 @@
     pair = lax.rem(y, 2)
     line = (z * 2 + pair) * s.C + c
 
-    def at(dz=0, dy=0, dc=0, dx=0, across=0):
+    z_pair = lax.rem(z, 2)
+    block = lax.div(z, 2)
+
+    def at(dz=0, dy=0, dc=0, dx=0, across=0, across_z=0):
         return (
-            lax.rem(z + dz, s.Z) if dz else z,
+            z + 1 - 2 * z_pair if across_z else lax.rem(z + dz, s.Z) if dz else z,
             y + 1 - 2 * pair if across else lax.rem(y + dy, s.Y) if dy else y,
             lax.rem(c + dc, s.C) if dc else c,
             lax.rem(x + dx, s.X) if dx else x,
@@ -155,7 +159,8 @@
     y_w = ordered((0, i, k, 0) for i in range(0, s.Y, 2) for k in range(s.C))
     y_c = ordered((0, i, k, 0) for i in range(s.Y) for k in range(s.C))
     z_only = ordered((i, 0, 0, 0) for i in range(s.Z))
-    z_x = ordered((i, 0, 0, j) for i in range(s.Z) for j in range(s.X))
+    z_even = ordered((i, 0, 0, 0) for i in range(0, s.Z, 2))
+    out_from = ordered((0, i, 0, 0, 0, k) for i in range(s.Y) for k in range(2))
     z_y = ordered((i, j, 0, 0) for i in range(s.Z) for j in range(s.Y))
     x_only = ordered((0, 0, 0, i) for i in range(s.X))
     partner = at(dc=1)
@@ -179,6 +184,9 @@
             device_id=partner,
             device_id_type=MESH,
         )
+
+    def side_of(its_z, its_y):
+        return (lax.rem(its_z, 2) * s.Y + its_y) * s.blocks + lax.div(its_z, 2)
 
     loads = []
 
@@ -199,23 +207,34 @@
     ld_residual = [load(residual, v_residual), load(norm_gain, v_norm_gain)]
     ld_ids = load(ids_t, v_ids)
     own_rows = pl.ds(pl.multiple_of(row * s.rows, s.rows), s.rows)
-    own_q = pl.ds(pl.multiple_of(x * s.dq, s.dq), s.dq)
+    chunk = s.chunk
+    wide_block = s.X * chunk
+
+    def chunk_of(i, j):
+        return pl.ds(pl.multiple_of(i * wide_block + j * chunk, chunk), chunk)
+
     own_f = pl.ds(pl.multiple_of(x * s.fh, s.fh), s.fh)
     own_f2 = pl.ds(pl.multiple_of(s.ff + x * s.fh, s.fh), s.fh)
     ld_state = [load(decay_bias, v_bias), load(head_gain, v_head_gain), load(state, v_state)]
     w_row[...] = jnp.zeros_like(w_row)
-    ld_out_w = [load(w_output_t, out_w.at[own_rows, :])]
+    v_group[...] = jnp.zeros_like(v_group)
+    out_slot = z_pair * s.Y + y
+    ld_out_w = [load(w_output_t, out_w.at[out_slot, c])]
     ld_ffn = [load(ffn_gain, v_ffn_gain)]
     ld_moe = [
-        load(w_gate.at[own_q, :], gate_w.at[:, own_f]),
-        load(w_up.at[own_q, :], gate_w.at[:, own_f2]),
-        load(w_down.at[:, own_q], down_w.at[own_f, :]),
-        load(router_expert.at[:, own_q], v_router),
-        load(router_group_t.at[:, own_q], v_group),
+        load(w_gate.at[:, x], gate_w.at[:, :, own_f]),
+        load(w_up.at[:, x], gate_w.at[:, :, own_f2]),
     ]
+    for i in range(s.blocks):
+        cols = pl.ds(i * chunk, chunk)
+        ld_moe.append(load(w_down.at[:, chunk_of(i, x)], down_w.at[own_f, cols]))
+        ld_moe.append(load(router_expert.at[:, chunk_of(i, x)], v_router.at[:, cols]))
+        ld_moe.append(
+            load(router_group_t.at[:, chunk_of(i, x)], v_group.at[pl.ds(0, s.groups), cols])
+        )
 
     barrier = pltpu.get_barrier_semaphore()
-    greeted = y_c + [o for o in z_p if o[0]] + x_only
+    greeted = y_c + [o for o in z_p if o[0]] + x_only + [o for o in out_from if o[1] and o[5]]
     for o in greeted:
         pl.semaphore_signal(barrier, inc=1, device_id=at(*o), device_id_type=MESH)
 
@@ -237,23 +256,29 @@
         send(PROJ_T, normed_out.at[to[0]], normed_in.at[line], to)
     for o in z_only:
         pl.semaphore_signal(plane_sem, inc=1, device_id=at(*o), device_id_type=MESH)
+    for o in z_even:
+        to = at(*o)
+        theirs = chunk_of(lax.div(to[0], 2), x)
+        send(RESIDUAL, v_residual.at[:, theirs], residual_in.at[block], to)
     ld_out_w[0].wait()
-    for o in y_c:
-        to = at(*o)
-        send(OUT_W, out_w.at[own_rows, :], out_w.at[own_rows, :], to)
+    for o in out_from:
+        send(OUT_W, out_w.at[out_slot, c], out_w.at[out_slot, c], at(*o))
     for o in x_only:
         to = at(*o)
-        their_q = pl.ds(pl.multiple_of(to[3] * s.dq, s.dq), s.dq)
-        send(GATE_W, w_gate.at[their_q, :], gate_w.at[:, own_f], to)
-        send(GATE_W, w_up.at[their_q, :], gate_w.at[:, own_f2], to)
+        send(GATE_W, w_gate.at[:, to[3]], gate_w.at[:, :, own_f], to)
+        send(GATE_W, w_up.at[:, to[3]], gate_w.at[:, :, own_f2], to)
     for o in x_only:
         to = at(*o)
-        their_q = pl.ds(pl.multiple_of(to[3] * s.dq, s.dq), s.dq)
-        send(DOWN_W, w_down.at[:, their_q], down_w.at[own_f, :], to)
+        for i in range(s.blocks):
+            cols = pl.ds(i * chunk, chunk)
+            send(DOWN_W, w_down.at[:, chunk_of(i, to[3])], down_w.at[own_f, cols], to)
 
     normed_in[line] = normed_out[z]
+    residual_in[block] = v_residual[:, chunk_of(block, x)]
     w_row[own_rows, :] = w_own[c]
 
+    for copy in ld_ffn:
+        copy.wait()
     ld_ids.wait()
     tokens = s.tokens
     ids = v_ids[...]
@@ -273,13 +298,25 @@
     side = tokens // 2
     p_row = lax.broadcasted_iota(jnp.int32, (tokens, side), 0)
     p_col = lax.broadcasted_iota(jnp.int32, (tokens, side), 1)
-    p_tok = 2 * p_col - lax.rem(p_col, 2)
+    per_z = s.Y * s.Z
+    p_y = lax.div(lax.rem(p_col, per_z), s.Z)
+    p_z = 2 * lax.div(lax.rem(p_col, s.Z), 2) + lax.div(p_col, per_z)
+    p_tok = (p_z * s.Y + p_y) * 2 * s.C + lax.rem(p_col, 2)
     slot_side = lax.broadcasted_iota(jnp.int32, (CAP, side), 0).astype(F32) + 1.0
     code_c = matmul(code.astype(BF16), (p_row == p_tok + 2 * c).astype(BF16))
     code_o = matmul(code.astype(BF16), (p_row == p_tok + 2 * other_c).astype(BF16))
     own_here = (slot_side == code_c[0:1]).astype(F32)
     par_here = (slot_side == code_c[1:2]).astype(F32)
     own_there = (slot_side == code_o[0:1]).astype(F32)
+    o_row = lax.broadcasted_iota(jnp.int32, (8, side), 0)
+    o_col = lax.broadcasted_iota(jnp.int32, (8, side), 1)
+    own_pick = (o_col == 2 * side_of(z, y) + o_row) & (o_row < 2)
+    gains = row_of(v_ffn_gain)
+    gain = jnp.zeros((1, s.dq), F32)
+    for j in range(s.X):
+        starts = [i * wide_block + j * chunk for i in range(s.blocks)]
+        piece = jnp.concatenate([gains[:, a : a + chunk] for a in starts], axis=1)
+        gain = gain + jnp.where(x == j, piece, 0.0)
     own_here_t = own_here.T.astype(BF16)
     own_there_t = own_there.T.astype(BF16)
 
@@ -314,75 +351,86 @@
         axis=0,
     )
     read_out = read_out + jnp.sum(query * key, axis=1, keepdims=True) * value
-    heads[z] = rms_scale(read_out, row_of(v_head_gain)).astype(BF16)
-    for o in z_only:
-        send(HEADS, heads.at[z], heads.at[z], at(*o))
+    heads[block] = rms_scale(read_out, row_of(v_head_gain)).astype(BF16)
+    for o in z_even:
+        send(HEADS, heads.at[block], heads.at[block], at(*o))
+    all_of(OUT_W, out_w.at[pl.ds(0, len(out_from)), 0]).wait_recv()
+    send(OUT_PAIR, out_w.at[:, c], out_w.at[:, c], partner)
     for i in range(2):
         carried = factors[:, 2 + i : 3 + i] * v_state[i]
         new_state[i] = carried + factors[:, 4 + i : 5 + i] * value[i : i + 1]
 
+    all_of(RESIDUAL, residual_in.at[pl.ds(0, len(z_even))]).wait_recv()
+    all_of(OUT_PAIR, out_w.at[:, 0]).wait_recv()
+    all_of(HEADS, heads.at[pl.ds(0, len(z_even))]).wait_recv()
+    part = matmul_t(heads[...].reshape(s.Z, s.dvh), out_w[...].reshape(wide_block, s.dvh))
+    part = part.astype(BF16)
+    for j in range(s.X):
+        head_out[j] = part[:, j * chunk : (j + 1) * chunk]
+    for o in x_only:
+        to = at(*o)
+        send(HEAD_SUM, head_out.at[to[3]], head_in.at[x], to)
+    head_in[x] = head_out[x]
     pl.semaphore_wait(plane_sem, len(z_only))
-    all_of(OUT_W, out_w.at[pl.ds(0, len(y_c) * s.rows), :]).wait_recv()
-    all_of(HEADS, heads.at[pl.ds(0, len(z_only))]).wait_recv()
-    part = matmul_t(heads[...].reshape(2 * s.Z, s.dvh), out_w[...])
-    head_out[...] = part.astype(BF16).reshape(s.Z, 2, s.zb)
-    for o in z_x:
-        to = at(*o)
-        send(HEAD_SUM, head_out.at[to[0]], head_in.at[z * s.X + x], to)
-    head_in[z * s.X + x] = head_out[z]
-    for copy in ld_ffn:
-        copy.wait()
-    all_of(HEAD_SUM, head_in.at[pl.ds(0, len(z_x))]).wait_recv()
-    blocks = []
-    for i in range(s.Z):
-        total = head_in[i * s.X].astype(F32)
-        for j in range(1, s.X):
-            total = total + head_in[i * s.X + j].astype(F32)
-        blocks.append(total)
-    hidden_res = v_residual[...].astype(F32) + jnp.concatenate(blocks, axis=1)
-    hidden_res = hidden_res.astype(BF16).astype(F32)
-    moe_rows = rms_scale(hidden_res, row_of(v_ffn_gain)).astype(BF16)
-    for i in range(s.X):
-        moe_in[i] = moe_rows[:, i * s.dq : (i + 1) * s.dq]
-        hidden_q[i] = hidden_res[:, i * s.dq : (i + 1) * s.dq]
-
-    gathered[plane] = moe_in[x]
+    all_of(HEAD_SUM, head_in.at[pl.ds(0, len(x_only))]).wait_recv()
+    attention = head_in[0].astype(F32)
+    for j in range(1, s.X):
+        attention = attention + head_in[j].astype(F32)
+    residual_rows = residual_in[...].reshape(s.Z, chunk).astype(F32)
+    gathered[plane] = (residual_rows + attention).astype(BF16)
+
     for o in z_y:
-        send(GATHER, moe_in.at[x], gathered.at[plane], at(*o))
+        send(GATHER, gathered.at[plane], gathered.at[plane], at(*o))
     for copy in ld_moe:
         copy.wait()
     all_of(GATHER, gathered.at[pl.ds(0, len(z_y))]).wait_recv()
-    rows = gathered[...].reshape(side, s.dq)
+    rows = jnp.concatenate(
+        [
+            gathered[pl.ds(2 * s.Y * i, 2 * s.Y)].reshape(side, chunk)
+            for i in range(s.blocks)
+        ],
+        axis=1,
+    )
     picked_out[...] = matmul(par_here.astype(BF16), rows).astype(BF16)
     send(PICKED, picked_out, picked_in, partner)
     picked = matmul(own_here.astype(BF16), rows)
-    all_of(GATE_W, gate_w.at[:, pl.ds(0, 2 * len(x_only) * s.fh)]).wait_recv()
+    own_hidden = matmul(own_pick.astype(BF16), rows)
+    all_of(GATE_W, gate_w.at[:, :, pl.ds(0, 2 * len(x_only) * s.fh)]).wait_recv()
     all_of(PICKED, picked_in).wait_recv()
-    picked = (picked + picked_in[...].astype(F32)).astype(BF16)
+    picked = picked + picked_in[...].astype(F32)
+    square = jnp.sum(picked * picked, axis=1, keepdims=True)
+    picked = (picked * gain).astype(BF16)
     wide = 2 * s.ff
-    partial[x, :, 0:wide] = matmul(picked, gate_w[...]).astype(BF16)
-    partial[x, :, wide : wide + s.experts] = matmul_t(picked, v_router[...]).astype(BF16)
-    groups = matmul_t(picked, v_group[...]).astype(BF16)
-    partial[x, :, wide + s.experts : wide + s.experts + s.groups] = groups
+    tail = wide + s.experts
+    partial[x, :, 0:wide] = matmul(picked, gate_w[...].reshape(s.dq, wide)).astype(BF16)
+    partial[x, :, wide:tail] = matmul_t(picked, v_router[...]).astype(BF16)
+    groups = matmul_t(picked, v_group[...])
+    g_lane = lax.broadcasted_iota(jnp.int32, groups.shape, 1)
+    high = square.astype(BF16).astype(F32)
+    groups = jnp.where(g_lane == s.groups, high, groups)
+    groups = jnp.where(g_lane == s.groups + 1, square - high, groups)
+    partial[x, :, tail : tail + 128] = groups.astype(BF16)
     for o in x_only:
         send(GATE_SUM, partial.at[x], partial.at[x], at(*o))
     all_of(DOWN_W, down_w.at[pl.ds(0, len(x_only) * s.fh), :]).wait_recv()
     all_of(GATE_SUM, partial.at[pl.ds(0, len(x_only))]).wait_recv()
-    both = jnp.sum(partial[:, :, 0:wide].astype(F32), axis=0)
+    groups = jnp.sum(partial[:, :, tail : tail + 128].astype(F32), axis=0)
+    squares = (g_lane == s.groups) | (g_lane == s.groups + 1)
+    square = jnp.sum(jnp.where(squares, groups, 0.0), axis=1, keepdims=True)
+    factor = lax.rsqrt(square / s.d + EPSILON)
+    groups = groups * factor
+    both = jnp.sum(partial[:, :, 0:wide].astype(F32), axis=0) * factor
     gate, up = both[:, : s.ff], both[:, s.ff :]
     hidden = (gate * (1.0 / (1.0 + jnp.exp(-gate))) * up).astype(BF16)
     output = matmul(hidden, down_w[...])
-    logits = jnp.sum(partial[:, :, wide : wide + s.experts].astype(F32), axis=0)
-    groups = jnp.sum(
-        partial[:, :, wide + s.experts : wide + s.experts + s.groups].astype(F32), axis=0
-    )
+    logits = jnp.sum(partial[:, :, wide:tail].astype(F32), axis=0) * factor
     lane = lax.broadcasted_iota(jnp.int32, logits.shape, 1)
     chosen = jnp.sum(jnp.where(lane == expert, logits, 0.0), axis=1, keepdims=True)
     against = jnp.sum(jnp.where(lane == rival_id, logits, 0.0), axis=1, keepdims=True)
-    g_lane = lax.broadcasted_iota(jnp.int32, groups.shape, 1)
     own_group = lax.div(expert, s.experts // s.groups)
     g_own = jnp.sum(jnp.where(g_lane == own_group, groups, 0.0), axis=1, keepdims=True)
-    share = 1.0 / jnp.sum(jnp.exp(groups - g_own), axis=1, keepdims=True)
+    shares = jnp.where(g_lane < s.groups, jnp.exp(groups - g_own), 0.0)
+    share = 1.0 / jnp.sum(shares, axis=1, keepdims=True)
     weight = share * (1.0 / (1.0 + jnp.exp(against - chosen)))
     scaled = (output * weight).astype(BF16)
 
@@ -394,26 +442,31 @@
     combine_out[...] = merged.reshape(side // 2, 2, s.dq)
     for o in z_y:
         to = at(*o)
-        send(COMBINE, combine_out.at[to[0] * s.Y + to[1]], combine_in.at[plane], to)
-    combine_in[plane] = combine_out[plane]
+        send(COMBINE, combine_out.at[side_of(to[0], to[1])], combine_in.at[plane], to)
+    combine_in[plane] = combine_out[side_of(z, y)]
     all_of(COMBINE, combine_in.at[pl.ds(0, len(z_y))]).wait_recv()
     moe_sum = jnp.sum(combine_in[...].astype(F32), axis=0)
-    quarters[x] = (hidden_q[x] + moe_sum).astype(BF16)
+    quarters[x] = (own_hidden[0:2] + moe_sum).astype(BF16)
     for o in x_only:
         send(QUARTERS, quarters.at[x], quarters.at[x], at(*o))
     all_of(QUARTERS, quarters.at[pl.ds(0, len(x_only))]).wait_recv()
-    for i in range(s.X):
-        layer_out[:, i * s.dq : (i + 1) * s.dq] = quarters[i]
+    for j in range(s.X):
+        quarter = quarters[j]
+        for i in range(s.blocks):
+            start = i * wide_block + j * chunk
+            layer_out[:, start : start + chunk] = quarter[:, i * chunk : (i + 1) * chunk]
 
     all_of(PROJ_W, w_row.at[pl.ds(0, len(y_w) * s.rows), :]).wait_send()
     all_of(PROJ_T, normed_in.at[pl.ds(0, len(z_p))]).wait_send()
-    all_of(OUT_W, out_w.at[pl.ds(0, len(y_c) * s.rows), :]).wait_send()
+    all_of(RESIDUAL, residual_in.at[pl.ds(0, len(z_even))]).wait_send()
+    all_of(OUT_W, out_w.at[pl.ds(0, len(out_from)), 0]).wait_send()
+    all_of(OUT_PAIR, out_w.at[:, 0]).wait_send()
     all_of(PROJ_SUM, sums_out.at[pl.ds(0, len(z_p))]).wait_send()
-    all_of(HEADS, heads.at[pl.ds(0, len(z_only))]).wait_send()
-    all_of(HEAD_SUM, head_in.at[pl.ds(0, len(z_x))]).wait_send()
+    all_of(HEADS, heads.at[pl.ds(0, len(z_even))]).wait_send()
+    all_of(HEAD_SUM, head_in.at[pl.ds(0, len(x_only))]).wait_send()
     all_of(GATHER, gathered.at[pl.ds(0, len(z_y))]).wait_send()
     all_of(PICKED, picked_out).wait_send()
-    all_of(GATE_W, gate_w.at[:, pl.ds(0, 2 * len(x_only) * s.fh)]).wait_send()
+    all_of(GATE_W, gate_w.at[:, :, pl.ds(0, 2 * len(x_only) * s.fh)]).wait_send()
     all_of(DOWN_W, down_w.at[pl.ds(0, len(x_only) * s.fh), :]).wait_send()
     all_of(GATE_SUM, partial.at[pl.ds(0, len(x_only))]).wait_send()
     all_of(MERGE, merge_out).wait_send()
@@ -453,23 +506,22 @@
         vmem((2, s.tokens), jnp.int32),
         vmem((2, s.dkh, s.dvh), F32),
         vmem((s.experts, s.dq), BF16),
-        vmem((s.groups, s.dq), BF16),
+        vmem((128, s.dq), BF16),
         vmem((2, s.rows, s.half), BF16),
         vmem((s.zb, s.half), BF16),
         vmem((s.Z, 2, s.zb), BF16),
         vmem((s.Z * 2 * s.C, 2, s.zb), BF16),
-        vmem((s.zb, s.dvh), BF16),
+        vmem((2 * s.Y, s.C, s.rows, s.dvh), BF16),
         vmem((s.Z * 2 * s.C, 2, s.half), BF16),
         vmem((2, s.Z * 2, 2, s.half), BF16),
-        vmem((s.Z, 2, s.dvh), BF16),
-        vmem((s.Z, 2, s.zb), BF16),
-        vmem((s.Z * s.X, 2, s.zb), BF16),
-        vmem((s.X, 2, s.dq), BF16),
-        vmem((s.X, 2, s.dq), F32),
-        vmem((side // 2, 2, s.dq), BF16),
+        vmem((s.blocks, 2, s.dvh), BF16),
+        vmem((s.X, s.Z, s.chunk), BF16),
+        vmem((s.X, s.Z, s.chunk), BF16),
+        vmem((s.blocks, 2, s.chunk), BF16),
+        vmem((s.Z * s.Y, s.Z, s.chunk), BF16),
         vmem((CAP, s.dq), BF16),
         vmem((CAP, s.dq), BF16),
-        vmem((s.dq, 2 * s.ff), BF16),
+        vmem((s.blocks, s.chunk, 2 * s.ff), BF16),
         vmem((s.ff, s.dq), BF16),
         vmem((s.X, CAP, 2 * s.ff + s.experts + 128), BF16),
         vmem((side, s.dq), BF16),
@@ -477,7 +529,7 @@
         vmem((side // 2, 2, s.dq), BF16),
         vmem((side // 2, 2, s.dq), BF16),
         vmem((s.X, 2, s.dq), BF16),
-        pltpu.SemaphoreType.DMA((18,)),
+        pltpu.SemaphoreType.DMA((32,)),
         pltpu.SemaphoreType.DMA((EXCHANGES,)),
         pltpu.SemaphoreType.DMA((EXCHANGES,)),
         pltpu.SemaphoreType.REGULAR,
@@ -497,8 +549,8 @@
         router_group.T,
         router_expert,
         expert_ids.T,
-        w_gate[0],
-        w_up[0],
+        w_gate.reshape(s.blocks, s.X, s.chunk, s.fh),
+        w_up.reshape(s.blocks, s.X, s.chunk, s.fh),
         w_down[0],
     )
     anywhere = pl.BlockSpec(memory_space=pl.ANY)
@@ -542,6 +594,8 @@
         rows=d // (Z * Y * C),
         zb=d // Z,
         dq=d // X,
+        blocks=Z // 2,
+        chunk=2 * d // (Z * X),
         dkh=dkh,
         dvh=dvh,
         half=(3 * dkh + dvh) // 2,

time: 66.7 us -> 64.8 us (0.972)
  Pallas kernels: 65.9 us -> 63.6 us
    pallas_call x1, Pallas kernels: 64.9 us -> 62.7 us  [on_device(): pl.pallas_call(functools.partial(layer_kernel, s), out_shape=(pltpu.VMEM(...]
where the time goes in v3:
time: 64.8 us; the launch traced here: 64.3 us
  Pallas kernels  63.6 us (98%)
  between operations  0.65 us (1%)
    pallas_call x1, Pallas kernels, on_device(): pl.pallas_call(functools.partial(layer_kernel, s), out_shape=(pltpu.VMEM(...  62.7 us

profile of v3, /device:TPU:1, one launch (start us, length us, event | category | flops | bytes accessed | tf_op | source)
XLA Modules:
  0.0 64.3 jit_solution(3118694881692594829)
XLA Ops:
  0.6 62.7 %layer.1 = (bf16[2,2048]{1,0:T(2,128)(2,1)S(1)}, f32[2,256,512]{2,1,0:T(8,128)S(1)}) custom-call(bf16[2,2048]{1,0:T(2,128)(2,1)} %residual.1, bf16[2048]{0:T(1024)(128)(2,1)} %norm_gain.1, bf16[16,256]{1,0:T(8,128)(2,1)} %w_query.1, bf16[16,256]{1,0:T(8,128)(2,1)} %w_key.1, bf16[16,512]{1,0:T(8,128)(2,1)} %w_value.1, bf16[16,256]{1,0:T(8,128)(2,1)} %w_decay.1, ...), custom_call_target="tpu_custom_call" | custom-call | tf_op jit(solution)/shard_map/layer/pallas_call | solution.py:557
  63.3 1.0 %store.1 = (bf16[2,2048]{1,0:T(2,128)(2,1)}, f32[2,256,512]{2,1,0:T(8,128)}) custom-call(bf16[2,2048]{1,0:T(2,128)(2,1)S(1)} %get-tuple-element.6.layer, f32[2,256,512]{2,1,0:T(8,128)S(1)} %get-tuple-element.7.state), custom_call_target="tpu_custom_call" | custom-call | tf_op jit(solution)/shard_map/store/pallas_call | solution.py:567

commit v4 on v3

--- a/solution.py
+++ b/solution.py
@@ -23,7 +23,9 @@
     PROJ_T,
     RESIDUAL,
     OUT_W,
+    OUT_Z,
     OUT_PAIR,
+    OUT_PAIR_Z,
     PROJ_SUM,
     HEADS,
     HEAD_SUM,
@@ -36,7 +38,7 @@
     COMBINE,
     QUARTERS,
     EXCHANGES,
-) = range(17)
+) = range(19)
 
 
 def rounds(n, offset):
@@ -160,7 +162,7 @@
     y_c = ordered((0, i, k, 0) for i in range(s.Y) for k in range(s.C))
     z_only = ordered((i, 0, 0, 0) for i in range(s.Z))
     z_even = ordered((i, 0, 0, 0) for i in range(0, s.Z, 2))
-    out_from = ordered((0, i, 0, 0, 0, k) for i in range(s.Y) for k in range(2))
+    y_only = ordered((0, i, 0, 0) for i in range(s.Y))
     z_y = ordered((i, j, 0, 0) for i in range(s.Z) for j in range(s.Y))
     x_only = ordered((0, 0, 0, i) for i in range(s.X))
     partner = at(dc=1)
@@ -205,6 +207,12 @@
         load(w_value, w_own.at[1, :, pl.ds(k // 2, s.dvh)]),
     ]
     ld_residual = [load(residual, v_residual), load(norm_gain, v_norm_gain)]
+    w_row[...] = jnp.zeros_like(w_row)
+    barrier = pltpu.get_barrier_semaphore()
+    greeted = ordered(y_c + [o for o in z_p if o[0]] + x_only)
+    for o in greeted:
+        pl.semaphore_signal(barrier, inc=1, device_id=at(*o), device_id_type=MESH)
+
     ld_ids = load(ids_t, v_ids)
     own_rows = pl.ds(pl.multiple_of(row * s.rows, s.rows), s.rows)
     chunk = s.chunk
@@ -216,7 +224,6 @@
     own_f = pl.ds(pl.multiple_of(x * s.fh, s.fh), s.fh)
     own_f2 = pl.ds(pl.multiple_of(s.ff + x * s.fh, s.fh), s.fh)
     ld_state = [load(decay_bias, v_bias), load(head_gain, v_head_gain), load(state, v_state)]
-    w_row[...] = jnp.zeros_like(w_row)
     v_group[...] = jnp.zeros_like(v_group)
     out_slot = z_pair * s.Y + y
     ld_out_w = [load(w_output_t, out_w.at[out_slot, c])]
@@ -233,36 +240,28 @@
             load(router_group_t.at[:, chunk_of(i, x)], v_group.at[pl.ds(0, s.groups), cols])
         )
 
-    barrier = pltpu.get_barrier_semaphore()
-    greeted = y_c + [o for o in z_p if o[0]] + x_only + [o for o in out_from if o[1] and o[5]]
-    for o in greeted:
-        pl.semaphore_signal(barrier, inc=1, device_id=at(*o), device_id_type=MESH)
-
-    for copy in ld_weights:
-        copy.wait()
-
-    pl.semaphore_wait(barrier, len(greeted))
-
-    for o in y_w:
-        to = at(*o)
-        send(PROJ_W, w_own.at[to[2]], w_row.at[own_rows, :], to)
     for copy in ld_residual:
         copy.wait()
     normed = rms_scale(v_residual[...].astype(F32), row_of(v_norm_gain)).astype(BF16)
     for i in range(s.Z):
         normed_out[i] = normed[:, i * s.zb : (i + 1) * s.zb]
+    for copy in ld_weights:
+        copy.wait()
+
+    pl.semaphore_wait(barrier, len(greeted))
+
     for o in z_p:
         to = at(*o)
         send(PROJ_T, normed_out.at[to[0]], normed_in.at[line], to)
+    for o in y_w:
+        to = at(*o)
+        send(PROJ_W, w_own.at[to[2]], w_row.at[own_rows, :], to)
     for o in z_only:
         pl.semaphore_signal(plane_sem, inc=1, device_id=at(*o), device_id_type=MESH)
     for o in z_even:
         to = at(*o)
         theirs = chunk_of(lax.div(to[0], 2), x)
         send(RESIDUAL, v_residual.at[:, theirs], residual_in.at[block], to)
-    ld_out_w[0].wait()
-    for o in out_from:
-        send(OUT_W, out_w.at[out_slot, c], out_w.at[out_slot, c], at(*o))
     for o in x_only:
         to = at(*o)
         send(GATE_W, w_gate.at[:, to[3]], gate_w.at[:, :, own_f], to)
@@ -276,6 +275,7 @@
     normed_in[line] = normed_out[z]
     residual_in[block] = v_residual[:, chunk_of(block, x)]
     w_row[own_rows, :] = w_own[c]
+    combine_in[plane] = jnp.zeros((2, s.dq), BF16)
 
     for copy in ld_ffn:
         copy.wait()
@@ -321,6 +321,9 @@
     own_there_t = own_there.T.astype(BF16)
 
     all_of(PROJ_T, normed_in.at[pl.ds(0, len(z_p))]).wait_recv()
+    ld_out_w[0].wait()
+    for o in y_only:
+        send(OUT_W, out_w.at[out_slot, c], out_w.at[out_slot, c], at(*o))
     all_of(PROJ_W, w_row.at[pl.ds(0, len(y_w) * s.rows), :]).wait_recv()
     lines = s.Z * 2 * s.C
     sums = matmul(normed_in[...].reshape(2 * lines, s.zb), w_row[...])
@@ -330,6 +333,11 @@
         to_line = (to[0] * 2 + lax.rem(to[1], 2)) * s.C + to[2]
         send(PROJ_SUM, sums_out.at[to_line], sums_in.at[c, z * 2 + pair], to)
     sums_in[c, z * 2 + pair] = sums_out[line]
+    here = pl.ds(pl.multiple_of(z_pair * s.Y, s.Y), s.Y)
+    there = pl.ds(pl.multiple_of((1 - z_pair) * s.Y, s.Y), s.Y)
+    all_of(OUT_W, out_w.at[pl.ds(0, len(y_only)), 0]).wait_recv()
+    send(OUT_Z, out_w.at[here].at[:, c], out_w.at[here].at[:, c], at(across_z=1))
+    send(OUT_PAIR, out_w.at[here].at[:, c], out_w.at[here].at[:, c], partner)
 
     for copy in ld_state:
         copy.wait()
@@ -354,14 +362,15 @@
     heads[block] = rms_scale(read_out, row_of(v_head_gain)).astype(BF16)
     for o in z_even:
         send(HEADS, heads.at[block], heads.at[block], at(*o))
-    all_of(OUT_W, out_w.at[pl.ds(0, len(out_from)), 0]).wait_recv()
-    send(OUT_PAIR, out_w.at[:, c], out_w.at[:, c], partner)
+    all_of(OUT_Z, out_w.at[pl.ds(0, s.Y), 0]).wait_recv()
+    send(OUT_PAIR_Z, out_w.at[there].at[:, c], out_w.at[there].at[:, c], partner)
     for i in range(2):
         carried = factors[:, 2 + i : 3 + i] * v_state[i]
         new_state[i] = carried + factors[:, 4 + i : 5 + i] * value[i : i + 1]
 
     all_of(RESIDUAL, residual_in.at[pl.ds(0, len(z_even))]).wait_recv()
-    all_of(OUT_PAIR, out_w.at[:, 0]).wait_recv()
+    all_of(OUT_PAIR, out_w.at[pl.ds(0, s.Y), 0]).wait_recv()
+    all_of(OUT_PAIR_Z, out_w.at[pl.ds(0, s.Y), 0]).wait_recv()
     all_of(HEADS, heads.at[pl.ds(0, len(z_even))]).wait_recv()
     part = matmul_t(heads[...].reshape(s.Z, s.dvh), out_w[...].reshape(wide_block, s.dvh))
     part = part.astype(BF16)
@@ -401,20 +410,25 @@
     square = jnp.sum(picked * picked, axis=1, keepdims=True)
     picked = (picked * gain).astype(BF16)
     wide = 2 * s.ff
-    tail = wide + s.experts
     partial[x, :, 0:wide] = matmul(picked, gate_w[...].reshape(s.dq, wide)).astype(BF16)
-    partial[x, :, wide:tail] = matmul_t(picked, v_router[...]).astype(BF16)
+    logits = matmul_t(picked, v_router[...])
     groups = matmul_t(picked, v_group[...])
+    lane = lax.broadcasted_iota(jnp.int32, logits.shape, 1)
+    ahead = jnp.where(lane == expert, logits, jnp.where(lane == rival_id, -logits, 0.0))
+    ahead = jnp.sum(ahead, axis=1, keepdims=True)
+    ahead_high = ahead.astype(BF16).astype(F32)
     g_lane = lax.broadcasted_iota(jnp.int32, groups.shape, 1)
     high = square.astype(BF16).astype(F32)
     groups = jnp.where(g_lane == s.groups, high, groups)
     groups = jnp.where(g_lane == s.groups + 1, square - high, groups)
-    partial[x, :, tail : tail + 128] = groups.astype(BF16)
+    groups = jnp.where(g_lane == s.groups + 2, ahead_high, groups)
+    groups = jnp.where(g_lane == s.groups + 3, ahead - ahead_high, groups)
+    partial[x, :, wide : wide + 128] = groups.astype(BF16)
     for o in x_only:
         send(GATE_SUM, partial.at[x], partial.at[x], at(*o))
     all_of(DOWN_W, down_w.at[pl.ds(0, len(x_only) * s.fh), :]).wait_recv()
     all_of(GATE_SUM, partial.at[pl.ds(0, len(x_only))]).wait_recv()
-    groups = jnp.sum(partial[:, :, tail : tail + 128].astype(F32), axis=0)
+    groups = jnp.sum(partial[:, :, wide : wide + 128].astype(F32), axis=0)
     squares = (g_lane == s.groups) | (g_lane == s.groups + 1)
     square = jnp.sum(jnp.where(squares, groups, 0.0), axis=1, keepdims=True)
     factor = lax.rsqrt(square / s.d + EPSILON)
@@ -423,15 +437,13 @@
     gate, up = both[:, : s.ff], both[:, s.ff :]
     hidden = (gate * (1.0 / (1.0 + jnp.exp(-gate))) * up).astype(BF16)
     output = matmul(hidden, down_w[...])
-    logits = jnp.sum(partial[:, :, wide:tail].astype(F32), axis=0) * factor
-    lane = lax.broadcasted_iota(jnp.int32, logits.shape, 1)
-    chosen = jnp.sum(jnp.where(lane == expert, logits, 0.0), axis=1, keepdims=True)
-    against = jnp.sum(jnp.where(lane == rival_id, logits, 0.0), axis=1, keepdims=True)
+    leads = (g_lane == s.groups + 2) | (g_lane == s.groups + 3)
+    ahead = jnp.sum(jnp.where(leads, groups, 0.0), axis=1, keepdims=True)
     own_group = lax.div(expert, s.experts // s.groups)
     g_own = jnp.sum(jnp.where(g_lane == own_group, groups, 0.0), axis=1, keepdims=True)
     shares = jnp.where(g_lane < s.groups, jnp.exp(groups - g_own), 0.0)
     share = 1.0 / jnp.sum(shares, axis=1, keepdims=True)
-    weight = share * (1.0 / (1.0 + jnp.exp(against - chosen)))
+    weight = share * (1.0 / (1.0 + jnp.exp(-ahead)))
     scaled = (output * weight).astype(BF16)
 
     merge_out[...] = matmul(own_there_t, scaled).astype(BF16)
@@ -439,28 +451,24 @@
     here = matmul(own_here_t, scaled)
     all_of(MERGE, merge_in).wait_recv()
     merged = (here + merge_in[...].astype(F32)).astype(BF16)
-    combine_out[...] = merged.reshape(side // 2, 2, s.dq)
+    combine_out[...] = merged
     for o in z_y:
         to = at(*o)
-        send(COMBINE, combine_out.at[side_of(to[0], to[1])], combine_in.at[plane], to)
-    combine_in[plane] = combine_out[side_of(z, y)]
+        theirs = pl.ds(pl.multiple_of(2 * side_of(to[0], to[1]), 2), 2)
+        send(COMBINE, combine_out.at[theirs, :], combine_in.at[plane], to)
+    own_moe = matmul(own_pick.astype(BF16), merged)
     all_of(COMBINE, combine_in.at[pl.ds(0, len(z_y))]).wait_recv()
-    moe_sum = jnp.sum(combine_in[...].astype(F32), axis=0)
+    moe_sum = own_moe[0:2] + jnp.sum(combine_in[...].astype(F32), axis=0)
     quarters[x] = (own_hidden[0:2] + moe_sum).astype(BF16)
     for o in x_only:
         send(QUARTERS, quarters.at[x], quarters.at[x], at(*o))
-    all_of(QUARTERS, quarters.at[pl.ds(0, len(x_only))]).wait_recv()
-    for j in range(s.X):
-        quarter = quarters[j]
-        for i in range(s.blocks):
-            start = i * wide_block + j * chunk
-            layer_out[:, start : start + chunk] = quarter[:, i * chunk : (i + 1) * chunk]
-
     all_of(PROJ_W, w_row.at[pl.ds(0, len(y_w) * s.rows), :]).wait_send()
     all_of(PROJ_T, normed_in.at[pl.ds(0, len(z_p))]).wait_send()
     all_of(RESIDUAL, residual_in.at[pl.ds(0, len(z_even))]).wait_send()
-    all_of(OUT_W, out_w.at[pl.ds(0, len(out_from)), 0]).wait_send()
-    all_of(OUT_PAIR, out_w.at[:, 0]).wait_send()
+    all_of(OUT_W, out_w.at[pl.ds(0, len(y_only)), 0]).wait_send()
+    all_of(OUT_Z, out_w.at[pl.ds(0, s.Y), 0]).wait_send()
+    all_of(OUT_PAIR, out_w.at[pl.ds(0, s.Y), 0]).wait_send()
+    all_of(OUT_PAIR_Z, out_w.at[pl.ds(0, s.Y), 0]).wait_send()
     all_of(PROJ_SUM, sums_out.at[pl.ds(0, len(z_p))]).wait_send()
     all_of(HEADS, heads.at[pl.ds(0, len(z_even))]).wait_send()
     all_of(HEAD_SUM, head_in.at[pl.ds(0, len(x_only))]).wait_send()
@@ -471,6 +479,12 @@
     all_of(GATE_SUM, partial.at[pl.ds(0, len(x_only))]).wait_send()
     all_of(MERGE, merge_out).wait_send()
     all_of(COMBINE, combine_in.at[pl.ds(0, len(z_y))]).wait_send()
+    all_of(QUARTERS, quarters.at[pl.ds(0, len(x_only))]).wait_recv()
+    for j in range(s.X):
+        quarter = quarters[j]
+        for i in range(s.blocks):
+            start = i * wide_block + j * chunk
+            layer_out[:, start : start + chunk] = quarter[:, i * chunk : (i + 1) * chunk]
     all_of(QUARTERS, quarters.at[pl.ds(0, len(x_only))]).wait_send()
 
 
@@ -523,10 +537,10 @@
         vmem((CAP, s.dq), BF16),
         vmem((s.blocks, s.chunk, 2 * s.ff), BF16),
         vmem((s.ff, s.dq), BF16),
-        vmem((s.X, CAP, 2 * s.ff + s.experts + 128), BF16),
+        vmem((s.X, CAP, 2 * s.ff + 128), BF16),
         vmem((side, s.dq), BF16),
         vmem((side, s.dq), BF16),
-        vmem((side // 2, 2, s.dq), BF16),
+        vmem((side, s.dq), BF16),
         vmem((side // 2, 2, s.dq), BF16),
         vmem((s.X, 2, s.dq), BF16),
         pltpu.SemaphoreType.DMA((32,)),

time: 64.8 us -> 62.3 us (0.961)
  Pallas kernels: 63.6 us -> 61.5 us
    pallas_call x1, Pallas kernels: 62.7 us -> 60.5 us  [on_device(): pl.pallas_call(functools.partial(layer_kernel, s), out_shape=(pltpu.VMEM(...]
where the time goes in v4:
time: 62.3 us; the launch traced here: 62.2 us
  Pallas kernels  61.5 us (99%)
  between operations  0.65 us (1%)
    pallas_call x1, Pallas kernels, on_device(): pl.pallas_call(functools.partial(layer_kernel, s), out_shape=(pltpu.VMEM(...  60.5 us

profile of v4, /device:TPU:1, one launch (start us, length us, event | category | flops | bytes accessed | tf_op | source)
XLA Modules:
  0.0 62.2 jit_solution(1830708573694766407)
XLA Ops:
  0.6 60.5 %layer.1 = (bf16[2,2048]{1,0:T(2,128)(2,1)S(1)}, f32[2,256,512]{2,1,0:T(8,128)S(1)}) custom-call(bf16[2,2048]{1,0:T(2,128)(2,1)} %residual.1, bf16[2048]{0:T(1024)(128)(2,1)} %norm_gain.1, bf16[16,256]{1,0:T(8,128)(2,1)} %w_query.1, bf16[16,256]{1,0:T(8,128)(2,1)} %w_key.1, bf16[16,512]{1,0:T(8,128)(2,1)} %w_value.1, bf16[16,256]{1,0:T(8,128)(2,1)} %w_decay.1, ...), custom_call_target="tpu_custom_call" | custom-call | tf_op jit(solution)/shard_map/layer/pallas_call | solution.py:571
  61.2 1.0 %store.1 = (bf16[2,2048]{1,0:T(2,128)(2,1)}, f32[2,256,512]{2,1,0:T(8,128)}) custom-call(bf16[2,2048]{1,0:T(2,128)(2,1)S(1)} %get-tuple-element.6.layer, f32[2,256,512]{2,1,0:T(8,128)S(1)} %get-tuple-element.7.state), custom_call_target="tpu_custom_call" | custom-call | tf_op jit(solution)/shard_map/store/pallas_call | solution.py:581
